TPU v7x, 32 devices: a whole 2x2x4 slice. The times are simulated.
32 devices in a mesh: sp: 16 (over z, y, x), tp: 2 (over core).
Axes of the slice: x: 2, y: 2, z: 4, core: 2. Of those that a mesh axis runs over, the one named last changes fastest.
Arguments:
- residual_in: bfloat16 [6144, 2048], P(('sp', 'tp')), may hold values from -6 to 6
- conv_values: bfloat16 [6144, 1024], P('sp', 'tp'), may hold values from -60 to 60
- conv_gates: bfloat16 [6144, 1024], P('sp', 'tp'), may hold values from -8 to 8
- conv_kernel: float32 [31, 1024], P(None, 'tp'), may hold values from -1 to 1
- conv_bias: float32 [1024], P('tp'), may hold values from -3 to 3
- chan_gain: float32 [1024], P('tp'), may hold values from 0.1 to 1.9
- chan_shift: float32 [1024], P('tp'), may hold values from -3 to 3
- out_weight: bfloat16 [1024, 2048], replicated, may hold values from -0.1875 to 0.1875
- norm_gain: float32 [2048], replicated, may hold values from 0.1 to 1.9
- route_ids: int32 [6144, 2], P(('sp', 'tp')), may hold values from 0 to 15, all different within a row; in each aligned block of 192 rows (0 to 191, 192 to 383, ...) at most 48 rows name the same one
- route_weights: float32 [6144, 2], P(('sp', 'tp')), may hold values from 0.25 to 1.5
- expert_gate: bfloat16 [16, 2048, 2048], P('sp', None, 'tp'), may hold values from -0.125 to 0.125
- expert_up: bfloat16 [16, 2048, 2048], P('sp', None, 'tp'), may hold values from -0.125 to 0.125
- expert_down: bfloat16 [16, 2048, 2048], P('sp', 'tp'), may hold values from -0.125 to 0.125
Outputs:
- layer_out: bfloat16 [6144, 2048], P(('sp', 'tp'))
Inputs may be any that keep to these rules, and one draw needn't show every extreme that they name: `route_ids`: each row names 2 different experts. Among the rows of one device (aligned blocks of 192 rows) no expert is named by more than 48 rows, a bound that some block reaches.
All inputs are finite; a program needn't handle non-finite values.
Results may differ from a plain program's by a relative error of at most 0.014.
Values may be sent and summed in bfloat16 or wider, within the bound.
A program may use at most 128 MiB of HBM per device.

v0:
```python
import functools

import jax
import jax.numpy as jnp
from jax import lax
from jax.experimental import pallas as pl
from jax.experimental.pallas import tpu as pltpu
from jax.sharding import PartitionSpec as P

GROUPS = 4
ORDER = (0, 2, 1, 3)
MESH = pl.DeviceIdType.MESH


def flipped(index, offset):
    result, bit = index, 1
    while bit <= offset:
        if offset & bit:
            result = result + bit * (1 - 2 * ((index // bit) % 2))
        bit *= 2
    return result


def experts_kernel(
    count, cap, send, gate_in, up_in, down_in, out,
    rows, part, given, total, hidden, gate_w, up_w, down_w,
    sent, came, back_sent, back_came, pair_sent, pair_came, part_sent, part_came, loaded,
):
    me, other = lax.axis_index("sp"), 1 - lax.axis_index("tp")
    per_group = count // GROUPS
    half = per_group * cap
    loads = [
        pltpu.make_async_copy(source.at[0], target, loaded.at[number])
        for number, (source, target) in enumerate(
            ((gate_in, gate_w), (up_in, up_w), (down_in, down_w))
        )
    ]
    for load in loads:
        load.start()

    barrier = pltpu.get_barrier_semaphore()
    for offset in range(1, count):
        pl.semaphore_signal(
            barrier, inc=1, device_id={"sp": flipped(me, offset)}, device_id_type=MESH
        )
    pl.semaphore_signal(barrier, inc=1, device_id={"tp": other}, device_id_type=MESH)
    pl.semaphore_wait(barrier, count)

    outgoing = {}
    for group in ORDER:
        for place in range(per_group):
            offset = group * per_group + place
            source = send.at[pl.ds(offset * cap, cap)]
            target = rows.at[group, pl.ds(place * cap, cap)]
            if offset == 0:
                copy = pltpu.make_async_copy(source, target, sent.at[0])
            else:
                copy = pltpu.make_async_remote_copy(
                    src_ref=source,
                    dst_ref=target,
                    send_sem=sent.at[offset],
                    recv_sem=came.at[offset],
                    device_id={"sp": flipped(me, offset)},
                    device_id_type=MESH,
                )
            copy.start()
            outgoing[offset] = copy

    late, returning = [], {}
    for turn, group in enumerate(ORDER):
        for place in range(per_group):
            offset = group * per_group + place
            if offset == 0:
                outgoing[0].wait()
            else:
                outgoing[offset].wait_recv()
        pair = pltpu.make_async_remote_copy(
            src_ref=rows.at[group, pl.ds(0, half)],
            dst_ref=rows.at[group, pl.ds(half, half)],
            send_sem=pair_sent.at[group],
            recv_sem=pair_came.at[group],
            device_id={"tp": other},
            device_id_type=MESH,
        )
        pair.start()
        late.append(pair)
        if turn == 0:
            for load in loads:
                load.wait()
        pair.wait_recv()

        wide = min(256, gate_w.shape[1])

        def first(step, carry, group=group):
            columns = pl.ds(pl.multiple_of(step * wide, wide), wide)
            gate = jnp.dot(rows[group], gate_w[:, columns], preferred_element_type=jnp.float32)
            upper = jnp.dot(rows[group], up_w[:, columns], preferred_element_type=jnp.float32)
            hidden[:, columns] = (jax.nn.silu(gate) * upper).astype(jnp.bfloat16)
            return carry

        lax.fori_loop(0, gate_w.shape[1] // wide, first, 0)

        def second(step, carry, group=group):
            columns = pl.ds(pl.multiple_of(step * wide, wide), wide)
            part[group, :, columns] = jnp.dot(
                hidden[...], down_w[:, columns], preferred_element_type=jnp.float32
            ).astype(jnp.bfloat16)
            return carry

        lax.fori_loop(0, down_w.shape[1] // wide, second, 0)

        share = pltpu.make_async_remote_copy(
            src_ref=part.at[group, pl.ds(half, half)],
            dst_ref=given.at[group],
            send_sem=part_sent.at[group],
            recv_sem=part_came.at[group],
            device_id={"tp": other},
            device_id_type=MESH,
        )
        share.start()
        late.append(share)
        share.wait_recv()
        total[group] = (
            part[group, pl.ds(0, half)].astype(jnp.float32) + given[group].astype(jnp.float32)
        ).astype(jnp.bfloat16)
        for place in range(per_group):
            offset = group * per_group + place
            source = total.at[group, pl.ds(place * cap, cap)]
            target = out.at[pl.ds(offset * cap, cap)]
            if offset == 0:
                copy = pltpu.make_async_copy(source, target, back_sent.at[0])
            else:
                copy = pltpu.make_async_remote_copy(
                    src_ref=source,
                    dst_ref=target,
                    send_sem=back_sent.at[offset],
                    recv_sem=back_came.at[offset],
                    device_id={"sp": flipped(me, offset)},
                    device_id_type=MESH,
                )
            copy.start()
            returning[offset] = copy

    for offset in range(1, count):
        outgoing[offset].wait_send()
    for copy in late:
        copy.wait_send()
    for offset in range(count):
        returning[offset].wait()


def run_experts(sendable, expert_gate, expert_up, expert_down, count, cap):
    width, units = expert_gate.shape[1], expert_gate.shape[2]
    half = count // GROUPS * cap
    grouped = pltpu.SemaphoreType.DMA((GROUPS,))
    each = pltpu.SemaphoreType.DMA((count,))
    vmem = pl.BlockSpec(memory_space=pltpu.VMEM)
    anywhere = pl.BlockSpec(memory_space=pl.ANY)
    held = jnp.bfloat16
    return pl.pallas_call(
        functools.partial(experts_kernel, count, cap),
        out_shape=jax.ShapeDtypeStruct(sendable.shape, held),
        in_specs=[vmem, anywhere, anywhere, anywhere],
        out_specs=vmem,
        scratch_shapes=[
            pltpu.VMEM((GROUPS, 2 * half, width), held),
            pltpu.VMEM((GROUPS, 2 * half, width), held),
            pltpu.VMEM((GROUPS, half, width), held),
            pltpu.VMEM((GROUPS, half, width), held),
            pltpu.VMEM((2 * half, units), held),
            pltpu.VMEM((width, units), held),
            pltpu.VMEM((width, units), held),
            pltpu.VMEM((units, width), held),
            each, each, each, each, grouped, grouped, grouped, grouped,
            pltpu.SemaphoreType.DMA((3,)),
        ],
        compiler_params=pltpu.CompilerParams(
            collective_id=0, has_side_effects=True, vmem_limit_bytes=60 * 1024 * 1024
        ),
    )(sendable, expert_gate, expert_up, expert_down)


def from_behind(value, axis, steps):
    count = lax.axis_size(axis)
    first, last = (max(0, -steps), min(count, count - steps))
    return lax.ppermute(value, axis, [(source, source + steps) for source in range(first, last)])


def swap(value, axis, offset):
    count = lax.axis_size(axis)
    return lax.ppermute(value, axis, [(source, source ^ offset) for source in range(count)])


def on_device(
    residual_in,
    conv_values,
    conv_gates,
    conv_kernel,
    conv_bias,
    chan_gain,
    chan_shift,
    out_weight,
    norm_gain,
    route_ids,
    route_weights,
    expert_gate,
    expert_up,
    expert_down,
):
    taps_count = conv_kernel.shape[0]
    tok_count, local_chan = conv_values.shape
    tp_count = lax.axis_size("tp")
    all_chan = local_chan * tp_count
    core = lax.axis_index("tp")
    gated = (
        conv_values.astype(jnp.float32) * jax.nn.sigmoid(conv_gates.astype(jnp.float32))
    ).astype(jnp.bfloat16)
    earlier = from_behind(gated[tok_count - (taps_count - 1) :], "sp", 1)
    extended = jnp.concatenate([earlier, gated], 0).astype(jnp.float32)
    mixed = jnp.zeros((tok_count, local_chan), jnp.float32) + conv_bias[None, :]
    for tap_index in range(taps_count):
        mixed = (
            mixed + conv_kernel[tap_index][None, :] * extended[tap_index : tap_index + tok_count]
        )
    sums = jnp.stack([jnp.sum(mixed, 1), jnp.sum(mixed * mixed, 1)])
    sums = sums + swap(sums, "tp", 1)
    center = (sums[0] / all_chan)[:, None]
    spread = (sums[1] / all_chan)[:, None] - center * center
    normed = (mixed - center) * lax.rsqrt(spread + 1e-06) * chan_gain[None, :] + chan_shift[None, :]
    activated = jax.nn.silu(normed).astype(jnp.bfloat16)
    row_count = tok_count // tp_count
    low, high = activated[:row_count], activated[row_count:]
    kept = jnp.where(core == 0, low, high)
    given = swap(jnp.where(core == 0, high, low), "tp", 1)
    regrouped = jnp.concatenate(
        [jnp.where(core == 0, kept, given), jnp.where(core == 0, given, kept)], 1
    )
    projected = jnp.dot(regrouped, out_weight, preferred_element_type=jnp.float32)
    after_f = (residual_in.astype(jnp.float32) + projected).astype(jnp.bfloat16).astype(jnp.float32)
    normal_rows = (
        after_f
        * lax.rsqrt(jnp.mean(after_f * after_f, 1, keepdims=True) + 1e-06)
        * norm_gain[None, :]
    ).astype(jnp.bfloat16)
    sp_count = lax.axis_size("sp")
    experts_all = expert_gate.shape[0] * sp_count
    choose_count = route_ids.shape[1]
    slot_cap = max(2, (2 * choose_count * row_count + experts_all - 1) // experts_all)
    slot_cap = (slot_cap + 15) // 16 * 16
    onehot = (
        route_ids.reshape(-1)[:, None] == jnp.arange(experts_all, dtype=jnp.int32)[None, :]
    ).astype(jnp.int32)
    before = jnp.cumsum(onehot, 0) - onehot
    ranking = jnp.sum(before * onehot, 1).reshape(row_count, choose_count)
    slot_ids = (route_ids ^ lax.axis_index("sp")) * slot_cap + ranking
    positions = lax.broadcasted_iota(jnp.int32, (experts_all * slot_cap, 1, 1), 0)
    dispatch = jnp.any(positions == slot_ids[None, :, :], axis=2).astype(jnp.bfloat16)
    columns = lax.broadcasted_iota(jnp.int32, (1, 1, experts_all * slot_cap), 2)
    weighting = jnp.sum(
        jnp.where(columns == slot_ids[:, :, None], route_weights[:, :, None], 0.0), 1
    )
    coarse_f = lax.reduce_precision(weighting, 8, 7)
    coarse = coarse_f.astype(jnp.bfloat16)
    fine = (weighting - coarse_f).astype(jnp.bfloat16)
    sendable = jnp.dot(dispatch, normal_rows, preferred_element_type=jnp.float32).astype(
        jnp.bfloat16
    )
    flat_out = run_experts(sendable, expert_gate, expert_up, expert_down, sp_count, slot_cap)
    combined = (
        after_f
        + jnp.dot(coarse, flat_out, preferred_element_type=jnp.float32)
        + jnp.dot(fine, flat_out, preferred_element_type=jnp.float32)
    )
    return combined.astype(jnp.bfloat16)


def solution(mesh):
    placed = (
        P(("sp", "tp"), None),
        P("sp", "tp"),
        P("sp", "tp"),
        P(None, "tp"),
        P("tp"),
        P("tp"),
        P("tp"),
        P(),
        P(),
        P(("sp", "tp"), None),
        P(("sp", "tp"), None),
        P("sp", None, "tp"),
        P("sp", None, "tp"),
        P("sp", "tp", None),
    )
    return jax.shard_map(
        on_device, mesh=mesh, in_specs=placed, out_specs=P(("sp", "tp"), None), check_vma=False
    )
```

profile of v0, /device:TPU:9, one launch (start us, length us, event | category | flops | bytes accessed | tf_op | source)
XLA Modules:
  0.0 177.5 jit_solution(1980439932750408297)
XLA Ops:
  0.0 0.0 copy-start.7
  0.0 1.4 multiply_convert_fusion.3
  1.4 3.1 %collective-permute-start = (bf16[30,512]{1,0:T(8,128)(2,1)S(1)}, bf16[30,512]{1,0:T(8,128)(2,1)S(1)}, u32[]{:S(2)}, u32[]{:S(2)}) collective-permute-start(bf16[30,512]{1,0:T(8,128)(2,1)S(1)} %slice.276), channel_id=1, source_target_pairs={{0,2},{2,4},{4,6},{6,8},{8,10},{10,12},{12,14},{14,16},{16,18},{18... | collective-permute-start | bytes 92168 | tf_op jit(solution)/shard_map/ppermute | solution.py:186
  4.5 1.1 fusion.52
  5.6 1.1 fusion.53
  6.7 0.8 copy.29
  7.5 0.1 eq.63
  7.6 0.1 eq.59
  7.8 0.9 reduce-window.6
  8.7 0.2 slice_reduce_fusion
  8.9 0.1 fusion.44
  9.0 0.1 reshape.61
  9.2 0.1 copy.32
  9.2 0.0 collective-permute-done
  9.2 0.1 maximum_convert_fusion
  9.4 0.0 copy-done.7
  9.4 0.0 copy-start.3
  9.4 0.0 copy-start.4
  9.4 0.0 copy-start.5
  9.4 3.8 %fusion.50 = (f32[384]{0:T(512)S(1)}, f32[384]{0:T(512)S(1)}, f32[384,512]{1,0:T(8,128)S(1)}) fusion(f32[414,512]{1,0:T(8,128)S(1)} %maximum_convert_fusion, f32[512]{0:T(512)S(1)} %bitcast.85, f32[512]{0:T(512)S(1)} %bitcast.86, f32[512]{0:T(512)S(1)} %bitcast.57, f32[512]{0:T(512)S(1)} %bitcast.58, f32[512]{0:T(512)S(1)} %bitcast.59, f32[512]{0:T(512)S(1)} %bitcast.60, ...), kind=kLoop, calls=%fused_computation.110 | loop fusion | flops 12778752 | bytes 25234432 | tf_op jit(solution)/shard_map/reduce_sum | solution.py:225
  13.3 0.0 copy-start.6
  13.3 1.0 collective-permute-start.1
  14.3 0.0 copy-done.3
  14.3 0.8 collective-permute-done.1
  15.2 0.0 copy-done.4
  15.2 0.0 copy-done.5
  15.2 0.0 copy-start.1
  15.2 0.4 multiply_convert_fusion.2
  15.6 0.4 collective-permute-start.2
  16.0 0.2 fusion.3
  16.2 0.0 copy-done.6
  16.2 0.2 select_reduce_fusion
  16.4 0.7 collective-permute-done.2
  17.2 0.0 copy-done.1
  17.2 0.0 copy-start.2
  17.2 3.4 %multiply_reduce_fusion = (f32[192]{0:T(256)S(1)}, f32[192,2048]{1,0:T(8,128)S(1)}) fusion(bf16[1024,2048]{1,0:T(8,128)(2,1)} %param.21, bf16[192,512]{1,0:T(8,128)(2,1)S(1)} %get-tuple-element.11, bf16[192,512]{1,0:T(8,128)(2,1)S(1)} %get-tuple-element.10, bf16[192,2048]{1,0:T(8,128)(2,1)S(1)} %copy-done.1), kind=kOutput, calls=%fused_computation.8 | convolution fusion | flops 808451904 | bytes 6947584 | tf_op jit(solution)/shard_map/dot_general | solution.py:238
  20.6 0.0 copy-done.2
  20.6 2.8 %convolution_convert_fusion.send = bf16[768,2048]{1,0:T(8,128)(2,1)} fusion(pred[768,192]{0,1:T(8,128)(4,1)S(1)} %fusion.3, f32[192,2048]{1,0:T(8,128)S(1)} %get-tuple-element.44, f32[2048]{0:T(1024)S(1)} %copy-done.2, f32[192]{0:T(256)S(1)} %add_rsqrt_fusion.1), kind=kOutput, calls=%fused_computation | convolution fusion | flops 606732288 | bytes 4875008 | tf_op jit(solution)/shard_map/dot_general | solution.py:265
  23.4 149.5 %shard_map.136 = bf16[768,2048]{1,0:T(8,128)(2,1)} custom-call(bf16[768,2048]{1,0:T(8,128)(2,1)} %convolution_convert_fusion.send, bf16[1,2048,1024]{2,1,0:T(8,128)(2,1)} %gate_in.1, bf16[1,2048,1024]{2,1,0:T(8,128)(2,1)} %up_in.1, bf16[1,1024,2048]{2,1,0:T(8,128)(2,1)} %down_in.1), custom_call_target="tpu_custom_call" | custom-call | tf_op jit(solution)/shard_map/pallas_call | solution.py:160
  172.9 0.0 copy-start
  173.0 2.8 %convolution_add_fusion.1 = f32[192,2048]{1,0:T(8,128)S(1)} fusion(f32[192,2048]{1,0:T(8,128)S(1)} %get-tuple-element.44, bf16[768,2048]{1,0:T(8,128)(2,1)} %shard_map.136, f32[192,768]{1,0:T(8,128)S(1)} %select_reduce_fusion), kind=kOutput, calls=%fused_computation.2 | convolution fusion | flops 604667904 | bytes 6881280 | tf_op jit(solution)/shard_map/dot_general | solution.py:271
  175.8 0.0 copy-done
  175.8 1.7 fusion.2
  (13 shorter events, 0.2 us)
Async XLA Ops:
  0.0 9.4 %copy-start.7 = (f32[512]{0:T(512)S(1)}, f32[512]{0:T(512)}, u32[]{:S(2)}) copy-start(f32[512]{0:T(512)} %param.18) | copy-start | bytes 6148
  1.4 7.9 %collective-permute-start = (bf16[30,512]{1,0:T(8,128)(2,1)S(1)}, bf16[30,512]{1,0:T(8,128)(2,1)S(1)}, u32[]{:S(2)}, u32[]{:S(2)}) collective-permute-start(bf16[30,512]{1,0:T(8,128)(2,1)S(1)} %slice.276), channel_id=1, source_target_pairs={{0,2},{2,4},{4,6},{6,8},{8,10},{10,12},{12,14},{14,16},{16,18},{18... | collective-permute-start | bytes 92168 | tf_op jit(solution)/shard_map/ppermute | solution.py:186
  9.4 4.9 %copy-start.3 = (s32[192,2]{0,1:T(2,128)S(1)}, s32[192,2]{0,1:T(2,128)}, u32[]{:S(2)}) copy-start(s32[192,2]{0,1:T(2,128)} %param.23) | copy-start | bytes 4612
  9.4 5.8 %copy-start.4 = (f32[512]{0:T(512)S(1)}, f32[512]{0:T(512)}, u32[]{:S(2)}) copy-start(f32[512]{0:T(512)} %param.20) | copy-start | bytes 6148
  9.4 5.8 %copy-start.5 = (f32[512]{0:T(512)S(1)}, f32[512]{0:T(512)}, u32[]{:S(2)}) copy-start(f32[512]{0:T(512)} %param.19) | copy-start | bytes 6148
  13.3 3.0 %copy-start.6 = (f32[192,2]{0,1:T(2,128)S(1)}, f32[192,2]{0,1:T(2,128)}, u32[]{:S(2)}) copy-start(f32[192,2]{0,1:T(2,128)} %param.24) | copy-start | bytes 4612
  13.3 1.8 %collective-permute-start.1 = (f32[2,384]{1,0:T(2,128)S(1)}, f32[2,384]{1,0:T(2,128)S(1)}, u32[]{:S(2)}, u32[]{:S(2)}) collective-permute-start(f32[2,384]{1,0:T(2,128)S(1)} %pad_maximum_fusion), channel_id=1, source_target_pairs={{0,1},{1,0},{2,3},{3,2},{4,5},{5,4},{6,7},{7,6},{8,9},{9,8},{10,11... | collective-permute-start | bytes 9224 | tf_op jit(solution)/shard_map/ppermute | solution.py:191
  15.2 2.0 %copy-start.1 = (bf16[192,2048]{1,0:T(8,128)(2,1)S(1)}, bf16[192,2048]{1,0:T(8,128)(2,1)}, u32[]{:S(2)}) copy-start(bf16[192,2048]{1,0:T(8,128)(2,1)} %param.14) | copy-start | bytes 2359300
  15.6 1.5 collective-permute-start.2
  17.2 3.4 %copy-start.2 = (f32[2048]{0:T(1024)S(1)}, f32[2048]{0:T(1024)}, u32[]{:S(2)}) copy-start(f32[2048]{0:T(1024)} %param.22) | copy-start | bytes 24580
  172.9 2.9 %copy-start = (bf16[768,2048]{1,0:T(8,128)(2,1)S(1)}, bf16[768,2048]{1,0:T(8,128)(2,1)}, u32[]{:S(2)}) copy-start(bf16[768,2048]{1,0:T(8,128)(2,1)} %shard_map.136) | copy-start | bytes 9437188
where the time goes:
time: 178 us
  Pallas kernels  150 us (84%)
  matrix products  10.7 us (6%)
  other arithmetic  7.16 us (4%)
  starting transfers between devices  4.55 us (3%)
  local copies, waits for them, and re-layouts  3.75 us (2%)
    pallas_call x1, Pallas kernels, run_experts(): pl.pallas_call(functools.partial(experts_kernel, count, cap), out_shape=j...  150 us
    reduce_sum x1, other arithmetic, on_device(): sums = jnp.stack([jnp.sum(mixed, 1), jnp.sum(mixed * mixed, 1)])  3.83 us
  transfers between devices with their start and end apart: 3, of which 2 were waited for; matrix products, arithmetic and copies ran while one was open for 3% of the time, Pallas kernels for 0%

commit v1 on v0

v1 whole, which is shorter than its diff:
```python
import functools

import jax
import jax.numpy as jnp
from jax import lax
from jax.experimental import pallas as pl
from jax.experimental.pallas import tpu as pltpu
from jax.sharding import PartitionSpec as P

PLANES = 4
CHUNKS = 4
MESH = pl.DeviceIdType.MESH


def flipped(index, offset):
    result, bit = index, 1
    while bit <= offset:
        if offset & bit:
            result = result + bit * (1 - 2 * ((index // bit) % 2))
        bit *= 2
    return result


def experts_kernel(
    count, cap, own, picks, weights, gate_in, up_in, down_in, out,
    dense, pick, rows, part, given, hidden, ret, zout, zin, gate_w, up_w, down_w,
    disp_sent, disp_came, plane_sent, plane_came, pair_sent, pair_came, part_sent, part_came,
    back_sent, back_came, chain_sent, chain_came, loaded,
):
    me, other = lax.axis_index("sp"), 1 - lax.axis_index("tp")
    chips = count // PLANES
    half = chips * cap
    z = me // chips
    mid = ((z + 1) // 2) % 2
    low = z // 2
    sources = (z, z + 1 - 2 * (z % 2), 2 - low, 3 * (1 - low))
    flips = (0, 1, 2 + mid, 3 - mid)
    ways = (0, 1 - 2 * (z % 2), 1 - 2 * low, 1 - 2 * low)
    landings = (
        0,
        sources[1] + (PLANES - sources[1]) * (z % 2),
        sources[2] + (PLANES - sources[2]) * low * (1 - z % 2),
        sources[3],
    )
    is_mid, is_end = mid == 1, mid == 0
    has_left, has_right = z > 0, z < PLANES - 1
    wide = own.shape[1] // CHUNKS

    def cols(number):
        return pl.ds(pl.multiple_of(number * wide, wide), wide)

    def along(way):
        return {"sp": me + way * chips}

    def dispatch(turn, way, slot):
        return pltpu.make_async_remote_copy(
            src_ref=own if turn == 0 else dense.at[sources[turn]],
            dst_ref=dense.at[sources[turn]],
            send_sem=disp_sent.at[turn, slot],
            recv_sem=disp_came.at[sources[turn]],
            device_id=along(way),
            device_id_type=MESH,
        )

    def plane_copy(turn, place):
        return pltpu.make_async_remote_copy(
            src_ref=pick.at[turn, pl.ds(place * cap, cap)],
            dst_ref=rows.at[turn, pl.ds(place * cap, cap)],
            send_sem=plane_sent.at[turn, place],
            recv_sem=plane_came.at[turn, place],
            device_id={"sp": flipped(me, place)},
            device_id_type=MESH,
        )

    def pair_copy(turn):
        return pltpu.make_async_remote_copy(
            src_ref=rows.at[turn, pl.ds(0, half)],
            dst_ref=rows.at[turn, pl.ds(half, half)],
            send_sem=pair_sent.at[turn],
            recv_sem=pair_came.at[turn],
            device_id={"tp": other},
            device_id_type=MESH,
        )

    def share_copy(turn, number):
        return pltpu.make_async_remote_copy(
            src_ref=part.at[turn, pl.ds(half, half), cols(number)],
            dst_ref=given.at[turn, :, cols(number)],
            send_sem=part_sent.at[turn, number],
            recv_sem=part_came.at[turn, number],
            device_id={"tp": other},
            device_id_type=MESH,
        )

    def back_copy(turn, number, place):
        return pltpu.make_async_remote_copy(
            src_ref=part.at[turn, pl.ds(place * cap, cap), cols(number)],
            dst_ref=ret.at[turn, pl.ds(place * cap, cap), cols(number)],
            send_sem=back_sent.at[turn, number, place],
            recv_sem=back_came.at[turn, number, place],
            device_id={"sp": flipped(me, place)},
            device_id_type=MESH,
        )

    def chain_copy(turn, number, landing=None):
        landing = landings[turn] if landing is None else landing
        return pltpu.make_async_remote_copy(
            src_ref=zout.at[turn, :, cols(number)],
            dst_ref=zin.at[landing, :, cols(number)],
            send_sem=chain_sent.at[turn, number],
            recv_sem=chain_came.at[landing, number],
            device_id=along(ways[turn]),
            device_id_type=MESH,
        )

    loads = [
        pltpu.make_async_copy(source.at[0], target, loaded.at[number])
        for number, (source, target) in enumerate(
            ((gate_in, gate_w), (up_in, up_w), (down_in, down_w))
        )
    ]
    for load in loads:
        load.start()

    barrier = pltpu.get_barrier_semaphore()
    for place in range(1, chips):
        pl.semaphore_signal(
            barrier, inc=1, device_id={"sp": flipped(me, place)}, device_id_type=MESH
        )
    pl.semaphore_signal(barrier, inc=1, device_id={"tp": other}, device_id_type=MESH)

    @pl.when(has_left)
    def _():
        pl.semaphore_signal(barrier, inc=1, device_id=along(-1), device_id_type=MESH)

    @pl.when(has_right)
    def _():
        pl.semaphore_signal(barrier, inc=1, device_id=along(1), device_id_type=MESH)

    pl.semaphore_wait(barrier, chips + (z + 2) // 3 + (PLANES + 1 - z) // 3)

    def send_own(way, slot):
        dispatch(0, way, slot).start()

    pl.when(has_left)(lambda: send_own(-1, 0))
    pl.when(has_right)(lambda: send_own(1, 1))

    def select(turn):
        block = own if turn == 0 else dense.at[sources[turn]]

        def step(number, carry):
            chosen = jnp.dot(
                picks[flips[turn]], block[:, cols(number)], preferred_element_type=jnp.float32
            ).astype(jnp.bfloat16)
            rows[turn, pl.ds(0, cap), cols(number)] = chosen[:cap]
            pick[turn, :, cols(number)] = chosen
            return carry

        lax.fori_loop(0, CHUNKS, step, 0)
        for place in range(1, chips):
            plane_copy(turn, place).start()

    def arrive(turn, forward):
        dispatch(turn, 0, 0).wait_recv()
        if forward:
            dispatch(turn, -ways[turn], 0).start()

    def expert(turn):
        for place in range(1, chips):
            plane_copy(turn, place).wait_recv()
        pair_copy(turn).start()
        if turn == 0:
            for load in loads:
                load.wait()
        pair_copy(turn).wait_recv()
        narrow = min(256, gate_w.shape[1])

        def first(step, carry):
            columns = pl.ds(pl.multiple_of(step * narrow, narrow), narrow)
            gate = jnp.dot(rows[turn], gate_w[:, columns], preferred_element_type=jnp.float32)
            upper = jnp.dot(rows[turn], up_w[:, columns], preferred_element_type=jnp.float32)
            hidden[:, columns] = (jax.nn.silu(gate) * upper).astype(jnp.bfloat16)
            return carry

        lax.fori_loop(0, gate_w.shape[1] // narrow, first, 0)

        def second(number, carry):
            part[turn, :, cols(number)] = jnp.dot(
                hidden[...], down_w[:, cols(number)], preferred_element_type=jnp.float32
            ).astype(jnp.bfloat16)
            share_copy(turn, number).start()
            return carry

        lax.fori_loop(0, CHUNKS, second, 0)

        def third(number, carry):
            share_copy(turn, number).wait_recv()
            total = (
                part[turn, pl.ds(0, half), cols(number)].astype(jnp.float32)
                + given[turn, :, cols(number)].astype(jnp.float32)
            ).astype(jnp.bfloat16)
            part[turn, pl.ds(0, half), cols(number)] = total
            ret[turn, pl.ds(0, cap), cols(number)] = total[:cap]
            for place in range(1, chips):
                back_copy(turn, number, place).start()
            return carry

        lax.fori_loop(0, CHUNKS, third, 0)

    def combined(turn, number):
        for place in range(1, chips):
            back_copy(turn, number, place).wait_recv()
        block = ret[turn, :, cols(number)]
        return jnp.dot(
            weights[flips[turn], 0], block, preferred_element_type=jnp.float32
        ) + jnp.dot(weights[flips[turn], 1], block, preferred_element_type=jnp.float32)

    def end_chain(turn):
        def step(number, carry):
            zout[turn, :, cols(number)] = combined(turn, number).astype(jnp.bfloat16)
            chain_copy(turn, number).start()
            return carry

        lax.fori_loop(0, CHUNKS, step, 0)

    def mid_link(turn, number):
        partial = combined(turn, number)
        chain_copy(turn, number, sources[turn]).wait_recv()
        zout[turn, :, cols(number)] = (
            partial + zin[sources[turn], :, cols(number)].astype(jnp.float32)
        ).astype(jnp.bfloat16)
        chain_copy(turn, number).start()

    select(0)
    expert(0)

    @pl.when(is_mid)
    def _():
        arrive(1, True)
        arrive(2, True)
        select(1)
        select(2)

    @pl.when(is_end)
    def _():
        arrive(1, False)
        select(1)

    expert(1)

    @pl.when(is_mid)
    def _():
        arrive(3, True)
        select(3)

    @pl.when(is_end)
    def _():
        arrive(2, False)
        select(2)
        end_chain(1)

    expert(2)

    @pl.when(is_end)
    def _():
        arrive(3, False)
        select(3)
        end_chain(2)

    expert(3)

    @pl.when(is_end)
    def _():
        end_chain(3)

    @pl.when(is_mid)
    def _():
        for number in range(CHUNKS):
            mid_link(2, number)
        mid_link(3, 0)
        for number in range(1, CHUNKS):
            mid_link(3, number)
            mid_link(1, number - 1)
        mid_link(1, CHUNKS - 1)

    def finish(number, carry):
        out[:, cols(number)] = combined(0, number)

        def joined(landing):
            chain_copy(1, number, landing).wait_recv()
            out[:, cols(number)] += zin[landing, :, cols(number)].astype(jnp.float32)

        pl.when(has_left)(lambda: joined(z))
        pl.when(has_right)(lambda: joined(PLANES))
        return carry

    lax.fori_loop(0, CHUNKS, finish, 0)

    pl.when(has_left)(lambda: dispatch(0, -1, 0).wait_send())
    pl.when(has_right)(lambda: dispatch(0, 1, 1).wait_send())

    @pl.when(is_mid)
    def _():
        for turn in range(1, PLANES):
            dispatch(turn, -ways[turn], 0).wait_send()

    for turn in range(PLANES):
        pair_copy(turn).wait_send()
        for place in range(1, chips):
            plane_copy(turn, place).wait_send()

        def drain(number, carry, turn=turn):
            share_copy(turn, number).wait_send()
            for place in range(1, chips):
                back_copy(turn, number, place).wait_send()
            if turn:
                chain_copy(turn, number).wait_send()
            return carry

        lax.fori_loop(0, CHUNKS, drain, 0)


def run_experts(own, picks, weights, expert_gate, expert_up, expert_down, count, cap):
    row_count, width = own.shape
    units = expert_gate.shape[2]
    chips = count // PLANES
    half = chips * cap
    dma = lambda *shape: pltpu.SemaphoreType.DMA(shape)
    vmem = pl.BlockSpec(memory_space=pltpu.VMEM)
    anywhere = pl.BlockSpec(memory_space=pl.ANY)
    held = jnp.bfloat16
    return pl.pallas_call(
        functools.partial(experts_kernel, count, cap),
        out_shape=jax.ShapeDtypeStruct((row_count, width), jnp.float32),
        in_specs=[vmem, vmem, vmem, anywhere, anywhere, anywhere],
        out_specs=vmem,
        scratch_shapes=[
            pltpu.VMEM((PLANES, row_count, width), held),
            pltpu.VMEM((PLANES, half, width), held),
            pltpu.VMEM((PLANES, 2 * half, width), held),
            pltpu.VMEM((PLANES, 2 * half, width), held),
            pltpu.VMEM((PLANES, half, width), held),
            pltpu.VMEM((2 * half, units), held),
            pltpu.VMEM((PLANES, half, width), held),
            pltpu.VMEM((PLANES, row_count, width), held),
            pltpu.VMEM((PLANES + 1, row_count, width), held),
            pltpu.VMEM((width, units), held),
            pltpu.VMEM((width, units), held),
            pltpu.VMEM((units, width), held),
            dma(PLANES, 2), dma(PLANES),
            dma(PLANES, chips), dma(PLANES, chips),
            dma(PLANES), dma(PLANES),
            dma(PLANES, CHUNKS), dma(PLANES, CHUNKS),
            dma(PLANES, CHUNKS, chips), dma(PLANES, CHUNKS, chips),
            dma(PLANES, CHUNKS), dma(PLANES + 1, CHUNKS),
            dma(3),
        ],
        compiler_params=pltpu.CompilerParams(
            collective_id=0, has_side_effects=True, vmem_limit_bytes=62 * 1024 * 1024
        ),
    )(own, picks, weights, expert_gate, expert_up, expert_down)


def from_behind(value, axis, steps):
    count = lax.axis_size(axis)
    first, last = (max(0, -steps), min(count, count - steps))
    return lax.ppermute(value, axis, [(source, source + steps) for source in range(first, last)])


def swap(value, axis, offset):
    count = lax.axis_size(axis)
    return lax.ppermute(value, axis, [(source, source ^ offset) for source in range(count)])


def on_device(
    residual_in,
    conv_values,
    conv_gates,
    conv_kernel,
    conv_bias,
    chan_gain,
    chan_shift,
    out_weight,
    norm_gain,
    route_ids,
    route_weights,
    expert_gate,
    expert_up,
    expert_down,
):
    taps_count = conv_kernel.shape[0]
    tok_count, local_chan = conv_values.shape
    tp_count = lax.axis_size("tp")
    all_chan = local_chan * tp_count
    core = lax.axis_index("tp")
    gated = (
        conv_values.astype(jnp.float32) * jax.nn.sigmoid(conv_gates.astype(jnp.float32))
    ).astype(jnp.bfloat16)
    earlier = from_behind(gated[tok_count - (taps_count - 1) :], "sp", 1)
    extended = jnp.concatenate([earlier, gated], 0).astype(jnp.float32)
    mixed = jnp.zeros((tok_count, local_chan), jnp.float32) + conv_bias[None, :]
    for tap_index in range(taps_count):
        mixed = (
            mixed + conv_kernel[tap_index][None, :] * extended[tap_index : tap_index + tok_count]
        )
    sums = jnp.stack([jnp.sum(mixed, 1), jnp.sum(mixed * mixed, 1)])
    sums = sums + swap(sums, "tp", 1)
    center = (sums[0] / all_chan)[:, None]
    spread = (sums[1] / all_chan)[:, None] - center * center
    normed = (mixed - center) * lax.rsqrt(spread + 1e-06) * chan_gain[None, :] + chan_shift[None, :]
    activated = jax.nn.silu(normed).astype(jnp.bfloat16)
    row_count = tok_count // tp_count
    low, high = activated[:row_count], activated[row_count:]
    kept = jnp.where(core == 0, low, high)
    given = swap(jnp.where(core == 0, high, low), "tp", 1)
    regrouped = jnp.concatenate(
        [jnp.where(core == 0, kept, given), jnp.where(core == 0, given, kept)], 1
    )
    projected = jnp.dot(regrouped, out_weight, preferred_element_type=jnp.float32)
    after_f = (residual_in.astype(jnp.float32) + projected).astype(jnp.bfloat16).astype(jnp.float32)
    normal_rows = (
        after_f
        * lax.rsqrt(jnp.mean(after_f * after_f, 1, keepdims=True) + 1e-06)
        * norm_gain[None, :]
    ).astype(jnp.bfloat16)
    sp_count = lax.axis_size("sp")
    experts_all = expert_gate.shape[0] * sp_count
    choose_count = route_ids.shape[1]
    slot_cap = max(2, (2 * choose_count * row_count + experts_all - 1) // experts_all)
    slot_cap = (slot_cap + 15) // 16 * 16
    onehot = (
        route_ids.reshape(-1)[:, None] == jnp.arange(experts_all, dtype=jnp.int32)[None, :]
    ).astype(jnp.int32)
    before = jnp.cumsum(onehot, 0) - onehot
    ranking = jnp.sum(before * onehot, 1).reshape(row_count, choose_count)
    chips = sp_count // PLANES
    half = chips * slot_cap
    me = lax.axis_index("sp")
    plane, place = me // chips, me % chips
    target_plane, target_place = route_ids // chips, route_ids % chips
    slot_ids = target_plane * half + (target_place ^ place) * slot_cap + ranking
    routing = jnp.concatenate([slot_ids.astype(jnp.float32), route_weights], 1).T
    routings = [routing] + [swap(routing, "sp", flip * chips) for flip in range(1, PLANES)]
    base = (plane * half).astype(jnp.float32)
    slots = lax.broadcasted_iota(jnp.int32, (half, 1), 0).astype(jnp.float32) + base
    lanes = lax.broadcasted_iota(jnp.int32, (1, half), 1).astype(jnp.float32) + base
    picks, weights = [], []
    for held in routings:
        ids, scales = held[:choose_count], held[choose_count:]
        chosen = functools.reduce(
            jnp.logical_or, [slots == ids[choice][None, :] for choice in range(choose_count)]
        )
        picks.append(chosen.astype(jnp.bfloat16))
        weighting = sum(
            jnp.where(lanes == ids[choice][:, None], scales[choice][:, None], 0.0)
            for choice in range(choose_count)
        )
        coarse_f = lax.reduce_precision(weighting, 8, 7)
        weights.append(
            jnp.stack([coarse_f.astype(jnp.bfloat16), (weighting - coarse_f).astype(jnp.bfloat16)])
        )
    summed = run_experts(
        normal_rows, jnp.stack(picks), jnp.stack(weights),
        expert_gate, expert_up, expert_down, sp_count, slot_cap,
    )
    combined = after_f + summed
    return combined.astype(jnp.bfloat16)


def solution(mesh):
    placed = (
        P(("sp", "tp"), None),
        P("sp", "tp"),
        P("sp", "tp"),
        P(None, "tp"),
        P("tp"),
        P("tp"),
        P("tp"),
        P(),
        P(),
        P(("sp", "tp"), None),
        P(("sp", "tp"), None),
        P("sp", None, "tp"),
        P("sp", None, "tp"),
        P("sp", "tp", None),
    )
    return jax.shard_map(
        on_device, mesh=mesh, in_specs=placed, out_specs=P(("sp", "tp"), None), check_vma=False
    )
```

time: 178 us -> 179 us (level)
  the two profiles are of different devices: /device:TPU:9 before, /device:TPU:0 now
where the time goes in v1:
time: 179 us; the launch traced here: 178 us
  Pallas kernels  149 us (83%)
  other arithmetic  14.5 us (8%)
  starting transfers between devices  9.56 us (5%)
  local copies, waits for them, and re-layouts  2.55 us (1%)
    pallas_call x1, Pallas kernels, run_experts(): pl.pallas_call(functools.partial(experts_kernel, count, cap), out_shape=j...  149 us
    ppermute x5, starting transfers between devices, swap(): lax.ppermute(value, axis, [(source, source ^ offset) for source in range(...  5.94 us
    reduce_sum x1, other arithmetic, on_device(): sums = jnp.stack([jnp.sum(mixed, 1), jnp.sum(mixed * mixed, 1)])  3.83 us
    ppermute x1, starting transfers between devices, from_behind(): lax.ppermute(value, axis, [(source, source + steps) for source in range(f...  3.62 us
  transfers between devices with their start and end apart: 6, of which 3 were waited for; matrix products, arithmetic and copies ran while one was open for 2% of the time, Pallas kernels for 0%

profile of v1, /device:TPU:0, one launch (start us, length us, event | category | flops | bytes accessed | tf_op | source)
XLA Modules:
  0.0 178.3 jit_solution(6269937677162629648)
XLA Ops:
  0.0 0.0 copy-start.2
  0.0 0.8 copy.48
  0.8 0.1 eq.381
  1.0 0.1 eq.377
  1.1 0.9 reduce-window.6
  2.0 0.2 slice_reduce_fusion
  2.3 0.1 fusion.42
  2.4 0.1 reshape.1692
  2.5 0.1 copy.51
  2.6 0.7 add_convert_fusion.2
  3.3 0.7 maximum_bitcast_fusion.4
  4.0 4.1 %collective-permute-start.4 = (f32[4,192]{1,0:T(4,128)S(1)}, f32[4,192]{1,0:T(4,128)S(1)}, u32[]{:S(2)}, u32[]{:S(2)}) collective-permute-start(f32[4,192]{1,0:T(4,128)S(1)} %maximum_bitcast_fusion.4), channel_id=1, source_target_pairs={{0,16},{2,18},{4,20},{6,22},{8,24},{10,26},{12,28},{14,30},{16,0},... | collective-permute-start | bytes 9224 | tf_op jit(solution)/shard_map/ppermute | solution.py:372
  8.1 1.6 collective-permute-start.3
  9.6 0.0 collective-permute-start.5
  9.6 1.3 multiply_convert_fusion.2
  11.0 3.6 %collective-permute-start = (bf16[30,512]{1,0:T(8,128)(2,1)S(1)}, bf16[30,512]{1,0:T(8,128)(2,1)S(1)}, u32[]{:S(2)}, u32[]{:S(2)}) collective-permute-start(bf16[30,512]{1,0:T(8,128)(2,1)S(1)} %slice.396), channel_id=1, source_target_pairs={{0,2},{2,4},{4,6},{6,8},{8,10},{10,12},{12,14},{14,16},{16,18},{18... | collective-permute-start | bytes 92168 | tf_op jit(solution)/shard_map/ppermute | solution.py:367
  14.6 0.0 copy-done.2
  14.7 0.0 copy-start.6
  14.8 0.0 collective-permute-done.4
  14.8 0.0 collective-permute-done.3
  14.8 0.2 collective-permute-done.5
  15.0 0.2 compare_or_fusion.3
  15.2 0.5 reduce-precision_convert_fusion.3
  15.7 0.8 add_convert_fusion.1.picks
  16.6 0.0 collective-permute-done
  16.6 0.1 maximum_convert_fusion
  16.7 0.0 copy-done.6
  16.7 0.0 copy-start.4
  16.7 0.0 copy-start.5
  16.7 3.8 %fusion.49 = (f32[384]{0:T(512)S(1)}, f32[384]{0:T(512)S(1)}, f32[384,512]{1,0:T(8,128)S(1)}) fusion(f32[414,512]{1,0:T(8,128)S(1)} %maximum_convert_fusion, f32[512]{0:T(512)S(1)} %bitcast.105, f32[512]{0:T(512)S(1)} %bitcast.106, f32[512]{0:T(512)S(1)} %bitcast.108, f32[512]{0:T(512)S(1)} %bitcast.109, f32[512]{0:T(512)S(1)} %bitcast.110, ...), kind=kLoop, calls=%fused_computation.132 | loop fusion | flops 12778752 | bytes 25234432 | tf_op jit(solution)/shard_map/reduce_sum | solution.py:406
  20.6 0.1 collective-permute-start.1
  20.7 0.1 maximum_bitcast_fusion
  20.8 1.1 collective-permute-done.1
  21.9 0.0 copy-done.4
  21.9 0.0 copy-done.5
  21.9 0.0 copy-start
  21.9 0.4 multiply_convert_fusion.1
  22.3 0.2 collective-permute-start.2
  22.5 0.0 copy-start.1
  22.5 0.1 maximum_bitcast_fusion.2
  22.6 1.1 pad_maximum_fusion.weights
  23.7 0.1 collective-permute-done.2
  23.9 0.5 copy-done
  24.4 0.4 copy-done.1
  24.7 0.0 copy-start.3
  24.7 1.1 multiply_reduce_fusion
  25.9 0.0 copy-done.3
  25.9 1.1 multiply_convert_fusion.own
  27.0 148.9 %shard_map.136 = f32[192,2048]{1,0:T(8,128)} custom-call(bf16[192,2048]{1,0:T(8,128)(2,1)} %multiply_convert_fusion.own, bf16[4,192,192]{2,1,0:T(8,128)(2,1)} %add_convert_fusion.1.picks, bf16[4,2,192,192]{3,2,1,0:T(8,128)(2,1)} %pad_maximum_fusion.weights, bf16[1,2048,1024]{2,1,0:T(8,128)(2,1)} %gate_in.1, bf16[1,2048,1024]{2,1,0:T(8,128)(2,1)} %up_in.1, ...), custom_call_target="tpu_custom_call" | custom-call | tf_op jit(solution)/shard_map/pallas_call | solution.py:332
  175.9 2.5 %add_convert_fusion = bf16[192,2048]{1,0:T(8,128)(2,1)} fusion(f32[192,2048]{1,0:T(8,128)S(1)} %get-tuple-element.78, f32[192,2048]{1,0:T(8,128)} %shard_map.136), kind=kLoop, calls=%fused_computation.3 | loop fusion | flops 786432 | bytes 3932160 | tf_op jit(solution)/shard_map/convert_element_type | solution.py:467
  (19 shorter events, 0.3 us)
Async XLA Ops:
  0.0 14.6 %copy-start.2 = (f32[31,512]{1,0:T(8,128)S(1)}, f32[31,512]{1,0:T(8,128)}, u32[]{:S(2)}) copy-start(f32[31,512]{1,0:T(8,128)} %param.17) | copy-start | bytes 190468
  4.0 10.8 %collective-permute-start.4 = (f32[4,192]{1,0:T(4,128)S(1)}, f32[4,192]{1,0:T(4,128)S(1)}, u32[]{:S(2)}, u32[]{:S(2)}) collective-permute-start(f32[4,192]{1,0:T(4,128)S(1)} %maximum_bitcast_fusion.4), channel_id=1, source_target_pairs={{0,16},{2,18},{4,20},{6,22},{8,24},{10,26},{12,28},{14,30},{16,0},... | collective-permute-start | bytes 9224 | tf_op jit(solution)/shard_map/ppermute | solution.py:372
  8.1 6.7 %collective-permute-start.3 = (f32[4,192]{1,0:T(4,128)S(1)}, f32[4,192]{1,0:T(4,128)S(1)}, u32[]{:S(2)}, u32[]{:S(2)}) collective-permute-start(f32[4,192]{1,0:T(4,128)S(1)} %maximum_bitcast_fusion.4), channel_id=1, source_target_pairs={{0,8},{2,10},{4,12},{6,14},{8,0},{10,2},{12,4},{14,6},{16,24},{18,... | collective-permute-start | bytes 9224 | tf_op jit(solution)/shard_map/ppermute | solution.py:372
  9.6 5.4 %collective-permute-start.5 = (f32[4,192]{1,0:T(4,128)S(1)}, f32[4,192]{1,0:T(4,128)S(1)}, u32[]{:S(2)}, u32[]{:S(2)}) collective-permute-start(f32[4,192]{1,0:T(4,128)S(1)} %maximum_bitcast_fusion.4), channel_id=1, source_target_pairs={{0,24},{2,26},{4,28},{6,30},{8,16},{10,18},{12,20},{14,22},{16,8},... | collective-permute-start | bytes 9224 | tf_op jit(solution)/shard_map/ppermute | solution.py:372
  11.0 5.6 %collective-permute-start = (bf16[30,512]{1,0:T(8,128)(2,1)S(1)}, bf16[30,512]{1,0:T(8,128)(2,1)S(1)}, u32[]{:S(2)}, u32[]{:S(2)}) collective-permute-start(bf16[30,512]{1,0:T(8,128)(2,1)S(1)} %slice.396), channel_id=1, source_target_pairs={{0,2},{2,4},{4,6},{6,8},{8,10},{10,12},{12,14},{14,16},{16,18},{18... | collective-permute-start | bytes 92168 | tf_op jit(solution)/shard_map/ppermute | solution.py:367
  14.7 2.0 %copy-start.6 = (f32[512]{0:T(512)S(1)}, f32[512]{0:T(512)}, u32[]{:S(2)}) copy-start(f32[512]{0:T(512)} %param.18) | copy-start | bytes 6148
  16.7 5.2 %copy-start.4 = (f32[512]{0:T(512)S(1)}, f32[512]{0:T(512)}, u32[]{:S(2)}) copy-start(f32[512]{0:T(512)} %param.20) | copy-start | bytes 6148
  16.7 5.2 %copy-start.5 = (f32[512]{0:T(512)S(1)}, f32[512]{0:T(512)}, u32[]{:S(2)}) copy-start(f32[512]{0:T(512)} %param.19) | copy-start | bytes 6148
  20.6 1.2 collective-permute-start.1
  21.9 2.5 %copy-start = (bf16[1024,2048]{1,0:T(8,128)(2,1)S(1)}, bf16[1024,2048]{1,0:T(8,128)(2,1)}, u32[]{:S(2)}) copy-start(bf16[1024,2048]{1,0:T(8,128)(2,1)} %param.21) | copy-start | bytes 12582916
  22.3 1.5 collective-permute-start.2
  22.5 2.2 %copy-start.1 = (bf16[192,2048]{1,0:T(8,128)(2,1)S(1)}, bf16[192,2048]{1,0:T(8,128)(2,1)}, u32[]{:S(2)}) copy-start(bf16[192,2048]{1,0:T(8,128)(2,1)} %param.14) | copy-start | bytes 2359300
  24.7 1.2 copy-start.3

commit v2 on v1

--- a/solution.py
+++ b/solution.py
@@ -52,32 +52,33 @@
     def along(way):
         return {"sp": me + way * chips}
 
-    def dispatch(turn, way, slot):
+    def dispatch(turn, number, way, slot):
+        block = own if turn == 0 else dense.at[sources[turn]]
         return pltpu.make_async_remote_copy(
-            src_ref=own if turn == 0 else dense.at[sources[turn]],
-            dst_ref=dense.at[sources[turn]],
-            send_sem=disp_sent.at[turn, slot],
-            recv_sem=disp_came.at[sources[turn]],
+            src_ref=block.at[:, cols(number)],
+            dst_ref=dense.at[sources[turn], :, cols(number)],
+            send_sem=disp_sent.at[turn, number, slot],
+            recv_sem=disp_came.at[sources[turn], number],
             device_id=along(way),
             device_id_type=MESH,
         )
 
-    def plane_copy(turn, place):
+    def plane_copy(turn, number, place):
         return pltpu.make_async_remote_copy(
-            src_ref=pick.at[turn, pl.ds(place * cap, cap)],
-            dst_ref=rows.at[turn, pl.ds(place * cap, cap)],
-            send_sem=plane_sent.at[turn, place],
-            recv_sem=plane_came.at[turn, place],
+            src_ref=pick.at[turn, pl.ds(place * cap, cap), cols(number)],
+            dst_ref=rows.at[turn, pl.ds(place * cap, cap), cols(number)],
+            send_sem=plane_sent.at[turn, number, place],
+            recv_sem=plane_came.at[turn, number, place],
             device_id={"sp": flipped(me, place)},
             device_id_type=MESH,
         )
 
-    def pair_copy(turn):
+    def pair_copy(turn, number):
         return pltpu.make_async_remote_copy(
-            src_ref=rows.at[turn, pl.ds(0, half)],
-            dst_ref=rows.at[turn, pl.ds(half, half)],
-            send_sem=pair_sent.at[turn],
-            recv_sem=pair_came.at[turn],
+            src_ref=rows.at[turn, pl.ds(0, half), cols(number)],
+            dst_ref=rows.at[turn, pl.ds(half, half), cols(number)],
+            send_sem=pair_sent.at[turn, number],
+            recv_sem=pair_came.at[turn, number],
             device_id={"tp": other},
             device_id_type=MESH,
         )
@@ -139,61 +140,71 @@
 
     pl.semaphore_wait(barrier, chips + (z + 2) // 3 + (PLANES + 1 - z) // 3)
 
-    def send_own(way, slot):
-        dispatch(0, way, slot).start()
-
-    pl.when(has_left)(lambda: send_own(-1, 0))
-    pl.when(has_right)(lambda: send_own(1, 1))
-
-    def select(turn):
+    def send_own(number, carry):
+        pl.when(has_left)(lambda: dispatch(0, number, -1, 0).start())
+        pl.when(has_right)(lambda: dispatch(0, number, 1, 1).start())
+        return carry
+
+    lax.fori_loop(0, CHUNKS, send_own, 0)
+
+    def select(turn, number):
         block = own if turn == 0 else dense.at[sources[turn]]
-
+        chosen = jnp.dot(
+            picks[flips[turn]], block[:, cols(number)], preferred_element_type=jnp.float32
+        ).astype(jnp.bfloat16)
+        rows[turn, pl.ds(0, cap), cols(number)] = chosen[:cap]
+        pick[turn, :, cols(number)] = chosen
+        for place in range(1, chips):
+            plane_copy(turn, number, place).start()
+
+    def arrive(turn, number, forward):
+        dispatch(turn, number, 0, 0).wait_recv()
+        if forward:
+            dispatch(turn, number, -ways[turn], 0).start()
+        select(turn, number)
+
+    def gather(turn):
         def step(number, carry):
-            chosen = jnp.dot(
-                picks[flips[turn]], block[:, cols(number)], preferred_element_type=jnp.float32
-            ).astype(jnp.bfloat16)
-            rows[turn, pl.ds(0, cap), cols(number)] = chosen[:cap]
-            pick[turn, :, cols(number)] = chosen
+            for place in range(1, chips):
+                plane_copy(turn, number, place).wait_recv()
+            pair_copy(turn, number).start()
             return carry
 
         lax.fori_loop(0, CHUNKS, step, 0)
-        for place in range(1, chips):
-            plane_copy(turn, place).start()
-
-    def arrive(turn, forward):
-        dispatch(turn, 0, 0).wait_recv()
-        if forward:
-            dispatch(turn, -ways[turn], 0).start()
-
-    def expert(turn):
-        for place in range(1, chips):
-            plane_copy(turn, place).wait_recv()
-        pair_copy(turn).start()
         if turn == 0:
             for load in loads:
                 load.wait()
-        pair_copy(turn).wait_recv()
+
+        def joined(number, carry):
+            pair_copy(turn, number).wait_recv()
+            return carry
+
+        lax.fori_loop(0, CHUNKS, joined, 0)
+
+    def first(turn):
         narrow = min(256, gate_w.shape[1])
 
-        def first(step, carry):
-            columns = pl.ds(pl.multiple_of(step * narrow, narrow), narrow)
+        def step(number, carry):
+            columns = pl.ds(pl.multiple_of(number * narrow, narrow), narrow)
             gate = jnp.dot(rows[turn], gate_w[:, columns], preferred_element_type=jnp.float32)
             upper = jnp.dot(rows[turn], up_w[:, columns], preferred_element_type=jnp.float32)
             hidden[:, columns] = (jax.nn.silu(gate) * upper).astype(jnp.bfloat16)
             return carry
 
-        lax.fori_loop(0, gate_w.shape[1] // narrow, first, 0)
-
-        def second(number, carry):
+        lax.fori_loop(0, gate_w.shape[1] // narrow, step, 0)
+
+    def second(turn):
+        def step(number, carry):
             part[turn, :, cols(number)] = jnp.dot(
                 hidden[...], down_w[:, cols(number)], preferred_element_type=jnp.float32
             ).astype(jnp.bfloat16)
             share_copy(turn, number).start()
             return carry
 
-        lax.fori_loop(0, CHUNKS, second, 0)
-
-        def third(number, carry):
+        lax.fori_loop(0, CHUNKS, step, 0)
+
+    def third(turn):
+        def step(number, carry):
             share_copy(turn, number).wait_recv()
             total = (
                 part[turn, pl.ds(0, half), cols(number)].astype(jnp.float32)
@@ -205,7 +216,7 @@
                 back_copy(turn, number, place).start()
             return carry
 
-        lax.fori_loop(0, CHUNKS, third, 0)
+        lax.fori_loop(0, CHUNKS, step, 0)
 
     def combined(turn, number):
         for place in range(1, chips):
@@ -231,47 +242,56 @@
         ).astype(jnp.bfloat16)
         chain_copy(turn, number).start()
 
-    select(0)
-    expert(0)
-
-    @pl.when(is_mid)
-    def _():
-        arrive(1, True)
-        arrive(2, True)
-        select(1)
-        select(2)
-
-    @pl.when(is_end)
-    def _():
-        arrive(1, False)
-        select(1)
-
-    expert(1)
-
-    @pl.when(is_mid)
-    def _():
-        arrive(3, True)
-        select(3)
-
-    @pl.when(is_end)
-    def _():
-        arrive(2, False)
-        select(2)
-        end_chain(1)
-
-    expert(2)
-
-    @pl.when(is_end)
-    def _():
-        arrive(3, False)
-        select(3)
-        end_chain(2)
-
-    expert(3)
-
-    @pl.when(is_end)
-    def _():
-        end_chain(3)
+    def at_mid(turn, begin, end):
+        @pl.when(is_mid)
+        def _():
+            for number in range(begin, end):
+                arrive(turn, number, True)
+
+    def at_end(turn, begin, end):
+        @pl.when(is_end)
+        def _():
+            for number in range(begin, end):
+                arrive(turn, number, False)
+
+    def near(begin, end):
+        for number in range(begin, end):
+            at_mid(1, number, number + 1)
+            at_mid(2, number, number + 1)
+            at_end(1, number, number + 1)
+
+    for number in range(CHUNKS):
+        select(0, number)
+    near(0, CHUNKS // 2)
+    gather(0)
+    first(0)
+    near(CHUNKS // 2, CHUNKS)
+    second(0)
+    at_mid(3, 0, CHUNKS // 4)
+    at_end(2, 0, CHUNKS // 4)
+    gather(1)
+    first(1)
+    at_mid(3, CHUNKS // 4, CHUNKS // 2)
+    at_end(2, CHUNKS // 4, CHUNKS // 2)
+    second(1)
+    third(1)
+    at_mid(3, CHUNKS // 2, CHUNKS)
+    at_end(2, CHUNKS // 2, CHUNKS)
+    pl.when(is_end)(lambda: end_chain(1))
+    at_end(3, 0, CHUNKS // 4)
+    gather(2)
+    first(2)
+    at_end(3, CHUNKS // 4, CHUNKS // 2)
+    second(2)
+    third(2)
+    at_end(3, CHUNKS // 2, CHUNKS)
+    pl.when(is_end)(lambda: end_chain(2))
+    third(0)
+    gather(3)
+    first(3)
+    second(3)
+    third(3)
+    pl.when(is_end)(lambda: end_chain(3))
 
     @pl.when(is_mid)
     def _():
@@ -296,28 +316,26 @@
 
     lax.fori_loop(0, CHUNKS, finish, 0)
 
-    pl.when(has_left)(lambda: dispatch(0, -1, 0).wait_send())
-    pl.when(has_right)(lambda: dispatch(0, 1, 1).wait_send())
-
-    @pl.when(is_mid)
-    def _():
-        for turn in range(1, PLANES):
-            dispatch(turn, -ways[turn], 0).wait_send()
-
-    for turn in range(PLANES):
-        pair_copy(turn).wait_send()
-        for place in range(1, chips):
-            plane_copy(turn, place).wait_send()
-
-        def drain(number, carry, turn=turn):
+    def drain(number, carry):
+        pl.when(has_left)(lambda: dispatch(0, number, -1, 0).wait_send())
+        pl.when(has_right)(lambda: dispatch(0, number, 1, 1).wait_send())
+
+        @pl.when(is_mid)
+        def _():
+            for turn in range(1, PLANES):
+                dispatch(turn, number, -ways[turn], 0).wait_send()
+
+        for turn in range(PLANES):
+            pair_copy(turn, number).wait_send()
             share_copy(turn, number).wait_send()
             for place in range(1, chips):
+                plane_copy(turn, number, place).wait_send()
                 back_copy(turn, number, place).wait_send()
             if turn:
                 chain_copy(turn, number).wait_send()
-            return carry
-
-        lax.fori_loop(0, CHUNKS, drain, 0)
+        return carry
+
+    lax.fori_loop(0, CHUNKS, drain, 0)
 
 
 def run_experts(own, picks, weights, expert_gate, expert_up, expert_down, count, cap):
@@ -347,9 +365,9 @@
             pltpu.VMEM((width, units), held),
             pltpu.VMEM((width, units), held),
             pltpu.VMEM((units, width), held),
-            dma(PLANES, 2), dma(PLANES),
-            dma(PLANES, chips), dma(PLANES, chips),
-            dma(PLANES), dma(PLANES),
+            dma(PLANES, CHUNKS, 2), dma(PLANES, CHUNKS),
+            dma(PLANES, CHUNKS, chips), dma(PLANES, CHUNKS, chips),
+            dma(PLANES, CHUNKS), dma(PLANES, CHUNKS),
             dma(PLANES, CHUNKS), dma(PLANES, CHUNKS),
             dma(PLANES, CHUNKS, chips), dma(PLANES, CHUNKS, chips),
             dma(PLANES, CHUNKS), dma(PLANES + 1, CHUNKS),

time: 179 us -> 153 us (0.85)
  Pallas kernels: 149 us -> 123 us
    pallas_call x1, Pallas kernels: 149 us -> 123 us  [run_experts(): pl.pallas_call(functools.partial(experts_kernel, count, cap), out_shape=j...]
  transfers between devices with their start and end apart: 6 -> 6, of which waited for: 3 -> 3; matrix products, arithmetic and copies ran while one was open for 2% -> 3% of each run, Pallas kernels for 0% -> 0%
where the time goes in v2:
time: 153 us
  Pallas kernels  123 us (80%)
  other arithmetic  14.5 us (9%)
  starting transfers between devices  9.56 us (6%)
  local copies, waits for them, and re-layouts  2.55 us (2%)
    pallas_call x1, Pallas kernels, run_experts(): pl.pallas_call(functools.partial(experts_kernel, count, cap), out_shape=j...  123 us
    ppermute x5, starting transfers between devices, swap(): lax.ppermute(value, axis, [(source, source ^ offset) for source in range(...  5.94 us
    reduce_sum x1, other arithmetic, on_device(): sums = jnp.stack([jnp.sum(mixed, 1), jnp.sum(mixed * mixed, 1)])  3.83 us
    ppermute x1, starting transfers between devices, from_behind(): lax.ppermute(value, axis, [(source, source + steps) for source in range(f...  3.62 us
  transfers between devices with their start and end apart: 6, of which 3 were waited for; matrix products, arithmetic and copies ran while one was open for 3% of the time, Pallas kernels for 0%

profile of v2, /device:TPU:0, one launch (start us, length us, event | category | flops | bytes accessed | tf_op | source)
XLA Modules:
  0.0 152.9 jit_solution(736282061822683799)
XLA Ops:
  0.0 0.0 copy-start.2
  0.0 0.8 copy.48
  0.8 0.1 eq.381
  1.0 0.1 eq.377
  1.1 0.9 reduce-window.6
  2.0 0.2 slice_reduce_fusion
  2.3 0.1 fusion.42
  2.4 0.1 reshape.1692
  2.5 0.1 copy.51
  2.6 0.7 add_convert_fusion.2
  3.3 0.7 maximum_bitcast_fusion.4
  4.0 4.1 %collective-permute-start.4 = (f32[4,192]{1,0:T(4,128)S(1)}, f32[4,192]{1,0:T(4,128)S(1)}, u32[]{:S(2)}, u32[]{:S(2)}) collective-permute-start(f32[4,192]{1,0:T(4,128)S(1)} %maximum_bitcast_fusion.4), channel_id=1, source_target_pairs={{0,16},{2,18},{4,20},{6,22},{8,24},{10,26},{12,28},{14,30},{16,0},... | collective-permute-start | bytes 9224 | tf_op jit(solution)/shard_map/ppermute | solution.py:390
  8.1 1.6 %collective-permute-start.3 = (f32[4,192]{1,0:T(4,128)S(1)}, f32[4,192]{1,0:T(4,128)S(1)}, u32[]{:S(2)}, u32[]{:S(2)}) collective-permute-start(f32[4,192]{1,0:T(4,128)S(1)} %maximum_bitcast_fusion.4), channel_id=1, source_target_pairs={{0,8},{2,10},{4,12},{6,14},{8,0},{10,2},{12,4},{14,6},{16,24},{18,... | collective-permute-start | bytes 9224 | tf_op jit(solution)/shard_map/ppermute | solution.py:390
  9.6 0.0 collective-permute-start.5
  9.6 1.3 multiply_convert_fusion.2
  11.0 3.6 %collective-permute-start = (bf16[30,512]{1,0:T(8,128)(2,1)S(1)}, bf16[30,512]{1,0:T(8,128)(2,1)S(1)}, u32[]{:S(2)}, u32[]{:S(2)}) collective-permute-start(bf16[30,512]{1,0:T(8,128)(2,1)S(1)} %slice.396), channel_id=1, source_target_pairs={{0,2},{2,4},{4,6},{6,8},{8,10},{10,12},{12,14},{14,16},{16,18},{18... | collective-permute-start | bytes 92168 | tf_op jit(solution)/shard_map/ppermute | solution.py:385
  14.6 0.0 copy-done.2
  14.7 0.0 copy-start.6
  14.8 0.0 collective-permute-done.4
  14.8 0.0 collective-permute-done.3
  14.8 0.2 collective-permute-done.5
  15.0 0.2 compare_or_fusion.3
  15.2 0.5 reduce-precision_convert_fusion.3
  15.7 0.8 add_convert_fusion.1.picks
  16.6 0.0 collective-permute-done
  16.6 0.1 maximum_convert_fusion
  16.7 0.0 copy-done.6
  16.7 0.0 copy-start.4
  16.7 0.0 copy-start.5
  16.7 3.8 %fusion.49 = (f32[384]{0:T(512)S(1)}, f32[384]{0:T(512)S(1)}, f32[384,512]{1,0:T(8,128)S(1)}) fusion(f32[414,512]{1,0:T(8,128)S(1)} %maximum_convert_fusion, f32[512]{0:T(512)S(1)} %bitcast.105, f32[512]{0:T(512)S(1)} %bitcast.106, f32[512]{0:T(512)S(1)} %bitcast.108, f32[512]{0:T(512)S(1)} %bitcast.109, f32[512]{0:T(512)S(1)} %bitcast.110, ...), kind=kLoop, calls=%fused_computation.132 | loop fusion | flops 12778752 | bytes 25234432 | tf_op jit(solution)/shard_map/reduce_sum | solution.py:424
  20.6 0.1 collective-permute-start.1
  20.7 0.1 maximum_bitcast_fusion
  20.8 1.1 collective-permute-done.1
  21.9 0.0 copy-done.4
  21.9 0.0 copy-done.5
  21.9 0.0 copy-start
  21.9 0.4 multiply_convert_fusion.1
  22.3 0.2 collective-permute-start.2
  22.5 0.0 copy-start.1
  22.5 0.1 maximum_bitcast_fusion.2
  22.6 1.1 pad_maximum_fusion.weights
  23.7 0.1 collective-permute-done.2
  23.9 0.5 copy-done
  24.4 0.4 copy-done.1
  24.7 0.0 copy-start.3
  24.7 1.1 multiply_reduce_fusion
  25.9 0.0 copy-done.3
  25.9 1.1 multiply_convert_fusion.own
  27.0 123.4 %shard_map.136 = f32[192,2048]{1,0:T(8,128)} custom-call(bf16[192,2048]{1,0:T(8,128)(2,1)} %multiply_convert_fusion.own, bf16[4,192,192]{2,1,0:T(8,128)(2,1)} %add_convert_fusion.1.picks, bf16[4,2,192,192]{3,2,1,0:T(8,128)(2,1)} %pad_maximum_fusion.weights, bf16[1,2048,1024]{2,1,0:T(8,128)(2,1)} %gate_in.1, bf16[1,2048,1024]{2,1,0:T(8,128)(2,1)} %up_in.1, ...), custom_call_target="tpu_custom_call" | custom-call | tf_op jit(solution)/shard_map/pallas_call | solution.py:350
  150.4 2.5 %add_convert_fusion = bf16[192,2048]{1,0:T(8,128)(2,1)} fusion(f32[192,2048]{1,0:T(8,128)S(1)} %get-tuple-element.78, f32[192,2048]{1,0:T(8,128)} %shard_map.136), kind=kLoop, calls=%fused_computation.3 | loop fusion | flops 786432 | bytes 3932160 | tf_op jit(solution)/shard_map/convert_element_type | solution.py:485
  (19 shorter events, 0.3 us)
Async XLA Ops:
  0.0 14.6 %copy-start.2 = (f32[31,512]{1,0:T(8,128)S(1)}, f32[31,512]{1,0:T(8,128)}, u32[]{:S(2)}) copy-start(f32[31,512]{1,0:T(8,128)} %param.17) | copy-start | bytes 190468
  4.0 10.8 %collective-permute-start.4 = (f32[4,192]{1,0:T(4,128)S(1)}, f32[4,192]{1,0:T(4,128)S(1)}, u32[]{:S(2)}, u32[]{:S(2)}) collective-permute-start(f32[4,192]{1,0:T(4,128)S(1)} %maximum_bitcast_fusion.4), channel_id=1, source_target_pairs={{0,16},{2,18},{4,20},{6,22},{8,24},{10,26},{12,28},{14,30},{16,0},... | collective-permute-start | bytes 9224 | tf_op jit(solution)/shard_map/ppermute | solution.py:390
  8.1 6.7 %collective-permute-start.3 = (f32[4,192]{1,0:T(4,128)S(1)}, f32[4,192]{1,0:T(4,128)S(1)}, u32[]{:S(2)}, u32[]{:S(2)}) collective-permute-start(f32[4,192]{1,0:T(4,128)S(1)} %maximum_bitcast_fusion.4), channel_id=1, source_target_pairs={{0,8},{2,10},{4,12},{6,14},{8,0},{10,2},{12,4},{14,6},{16,24},{18,... | collective-permute-start | bytes 9224 | tf_op jit(solution)/shard_map/ppermute | solution.py:390
  9.6 5.4 %collective-permute-start.5 = (f32[4,192]{1,0:T(4,128)S(1)}, f32[4,192]{1,0:T(4,128)S(1)}, u32[]{:S(2)}, u32[]{:S(2)}) collective-permute-start(f32[4,192]{1,0:T(4,128)S(1)} %maximum_bitcast_fusion.4), channel_id=1, source_target_pairs={{0,24},{2,26},{4,28},{6,30},{8,16},{10,18},{12,20},{14,22},{16,8},... | collective-permute-start | bytes 9224 | tf_op jit(solution)/shard_map/ppermute | solution.py:390
  11.0 5.6 %collective-permute-start = (bf16[30,512]{1,0:T(8,128)(2,1)S(1)}, bf16[30,512]{1,0:T(8,128)(2,1)S(1)}, u32[]{:S(2)}, u32[]{:S(2)}) collective-permute-start(bf16[30,512]{1,0:T(8,128)(2,1)S(1)} %slice.396), channel_id=1, source_target_pairs={{0,2},{2,4},{4,6},{6,8},{8,10},{10,12},{12,14},{14,16},{16,18},{18... | collective-permute-start | bytes 92168 | tf_op jit(solution)/shard_map/ppermute | solution.py:385
  14.7 2.0 %copy-start.6 = (f32[512]{0:T(512)S(1)}, f32[512]{0:T(512)}, u32[]{:S(2)}) copy-start(f32[512]{0:T(512)} %param.18) | copy-start | bytes 6148
  16.7 5.2 %copy-start.4 = (f32[512]{0:T(512)S(1)}, f32[512]{0:T(512)}, u32[]{:S(2)}) copy-start(f32[512]{0:T(512)} %param.20) | copy-start | bytes 6148
  16.7 5.2 %copy-start.5 = (f32[512]{0:T(512)S(1)}, f32[512]{0:T(512)}, u32[]{:S(2)}) copy-start(f32[512]{0:T(512)} %param.19) | copy-start | bytes 6148
  20.6 1.2 collective-permute-start.1
  21.9 2.5 %copy-start = (bf16[1024,2048]{1,0:T(8,128)(2,1)S(1)}, bf16[1024,2048]{1,0:T(8,128)(2,1)}, u32[]{:S(2)}) copy-start(bf16[1024,2048]{1,0:T(8,128)(2,1)} %param.21) | copy-start | bytes 12582916
  22.3 1.5 collective-permute-start.2
  22.5 2.2 %copy-start.1 = (bf16[192,2048]{1,0:T(8,128)(2,1)S(1)}, bf16[192,2048]{1,0:T(8,128)(2,1)}, u32[]{:S(2)}) copy-start(bf16[192,2048]{1,0:T(8,128)(2,1)} %param.14) | copy-start | bytes 2359300
  24.7 1.2 copy-start.3

commit v3 on v2

--- a/solution.py
+++ b/solution.py
@@ -8,7 +8,7 @@
 from jax.sharding import PartitionSpec as P
 
 PLANES = 4
-CHUNKS = 4
+CHUNKS = 8
 MESH = pl.DeviceIdType.MESH
 
 
@@ -43,42 +43,47 @@
         sources[3],
     )
     is_mid, is_end = mid == 1, mid == 0
+    crossed = (z, z + 1 - 2 * (z % 2), z + 2 - 4 * low, PLANES - 1 - z)
+    aways = (0, 2 * (z % 2) - 1, 2 * low - 1, 2 * low - 1)
     has_left, has_right = z > 0, z < PLANES - 1
     wide = own.shape[1] // CHUNKS
 
     def cols(number):
         return pl.ds(pl.multiple_of(number * wide, wide), wide)
 
+    def every(number):
+        return pl.ds(0, CHUNKS * wide) if number is None else cols(number)
+
     def along(way):
         return {"sp": me + way * chips}
 
-    def dispatch(turn, number, way, slot):
-        block = own if turn == 0 else dense.at[sources[turn]]
+    def dispatch(source, number, way, slot, block=None):
+        block = dense.at[source] if block is None else block
         return pltpu.make_async_remote_copy(
             src_ref=block.at[:, cols(number)],
-            dst_ref=dense.at[sources[turn], :, cols(number)],
-            send_sem=disp_sent.at[turn, number, slot],
-            recv_sem=disp_came.at[sources[turn], number],
+            dst_ref=dense.at[source, :, cols(number)],
+            send_sem=disp_sent.at[slot],
+            recv_sem=disp_came.at[source, number],
             device_id=along(way),
             device_id_type=MESH,
         )
 
-    def plane_copy(turn, number, place):
-        return pltpu.make_async_remote_copy(
-            src_ref=pick.at[turn, pl.ds(place * cap, cap), cols(number)],
-            dst_ref=rows.at[turn, pl.ds(place * cap, cap), cols(number)],
-            send_sem=plane_sent.at[turn, number, place],
-            recv_sem=plane_came.at[turn, number, place],
+    def plane_copy(turn, number, place, places=1):
+        return pltpu.make_async_remote_copy(
+            src_ref=pick.at[turn, pl.ds(place * cap, places * cap), cols(number)],
+            dst_ref=rows.at[turn, pl.ds(place * cap, places * cap), cols(number)],
+            send_sem=plane_sent.at[0],
+            recv_sem=plane_came.at[turn, number],
             device_id={"sp": flipped(me, place)},
             device_id_type=MESH,
         )
 
     def pair_copy(turn, number):
         return pltpu.make_async_remote_copy(
-            src_ref=rows.at[turn, pl.ds(0, half), cols(number)],
-            dst_ref=rows.at[turn, pl.ds(half, half), cols(number)],
-            send_sem=pair_sent.at[turn, number],
-            recv_sem=pair_came.at[turn, number],
+            src_ref=rows.at[turn, pl.ds(0, half), every(number)],
+            dst_ref=rows.at[turn, pl.ds(half, half), every(number)],
+            send_sem=pair_sent.at[0],
+            recv_sem=pair_came.at[turn],
             device_id={"tp": other},
             device_id_type=MESH,
         )
@@ -87,18 +92,18 @@
         return pltpu.make_async_remote_copy(
             src_ref=part.at[turn, pl.ds(half, half), cols(number)],
             dst_ref=given.at[turn, :, cols(number)],
-            send_sem=part_sent.at[turn, number],
+            send_sem=part_sent.at[0],
             recv_sem=part_came.at[turn, number],
             device_id={"tp": other},
             device_id_type=MESH,
         )
 
-    def back_copy(turn, number, place):
-        return pltpu.make_async_remote_copy(
-            src_ref=part.at[turn, pl.ds(place * cap, cap), cols(number)],
-            dst_ref=ret.at[turn, pl.ds(place * cap, cap), cols(number)],
-            send_sem=back_sent.at[turn, number, place],
-            recv_sem=back_came.at[turn, number, place],
+    def back_copy(turn, number, place, places=1):
+        return pltpu.make_async_remote_copy(
+            src_ref=part.at[turn, pl.ds(place * cap, places * cap), cols(number)],
+            dst_ref=ret.at[turn, pl.ds(place * cap, places * cap), cols(number)],
+            send_sem=back_sent.at[0],
+            recv_sem=back_came.at[turn, number],
             device_id={"sp": flipped(me, place)},
             device_id_type=MESH,
         )
@@ -108,7 +113,7 @@
         return pltpu.make_async_remote_copy(
             src_ref=zout.at[turn, :, cols(number)],
             dst_ref=zin.at[landing, :, cols(number)],
-            send_sem=chain_sent.at[turn, number],
+            send_sem=chain_sent.at[0],
             recv_sem=chain_came.at[landing, number],
             device_id=along(ways[turn]),
             device_id_type=MESH,
@@ -141,32 +146,40 @@
     pl.semaphore_wait(barrier, chips + (z + 2) // 3 + (PLANES + 1 - z) // 3)
 
     def send_own(number, carry):
-        pl.when(has_left)(lambda: dispatch(0, number, -1, 0).start())
-        pl.when(has_right)(lambda: dispatch(0, number, 1, 1).start())
+        pl.when(has_left)(lambda: dispatch(z, number, -1, 0, own).start())
+        pl.when(has_right)(lambda: dispatch(z, number, 1, 1, own).start())
         return carry
 
     lax.fori_loop(0, CHUNKS, send_own, 0)
 
-    def select(turn, number):
-        block = own if turn == 0 else dense.at[sources[turn]]
+    def select(turn, flip, block, number):
         chosen = jnp.dot(
-            picks[flips[turn]], block[:, cols(number)], preferred_element_type=jnp.float32
+            picks[flip], block[:, cols(number)], preferred_element_type=jnp.float32
         ).astype(jnp.bfloat16)
         rows[turn, pl.ds(0, cap), cols(number)] = chosen[:cap]
         pick[turn, :, cols(number)] = chosen
         for place in range(1, chips):
             plane_copy(turn, number, place).start()
 
-    def arrive(turn, number, forward):
-        dispatch(turn, number, 0, 0).wait_recv()
-        if forward:
-            dispatch(turn, number, -ways[turn], 0).start()
-        select(turn, number)
+    def arrive(turn, flip, number):
+        source = crossed[flip]
+        dispatch(source, number, 0, 0).wait_recv()
+        pl.when(is_mid)(lambda: dispatch(source, number, aways[flip], 2).start())
+        select(turn, flip, dense.at[source], number)
+
+    def near(number):
+        arrive(1, 1, number)
+        pl.when(is_mid)(lambda: arrive(2, 3, number))
+
+    def next_near(number):
+        arrive(2 + mid, 2, number)
+
+    def far(number):
+        pl.when(is_end)(lambda: arrive(3, 3, number))
 
     def gather(turn):
         def step(number, carry):
-            for place in range(1, chips):
-                plane_copy(turn, number, place).wait_recv()
+            plane_copy(turn, number, 1, chips - 1).wait_recv()
             pair_copy(turn, number).start()
             return carry
 
@@ -175,13 +188,9 @@
             for load in loads:
                 load.wait()
 
-        def joined(number, carry):
-            pair_copy(turn, number).wait_recv()
-            return carry
-
-        lax.fori_loop(0, CHUNKS, joined, 0)
-
-    def first(turn):
+        pair_copy(turn, None).wait_recv()
+
+    def first(turn, begin, end):
         narrow = min(256, gate_w.shape[1])
 
         def step(number, carry):
@@ -191,9 +200,10 @@
             hidden[:, columns] = (jax.nn.silu(gate) * upper).astype(jnp.bfloat16)
             return carry
 
-        lax.fori_loop(0, gate_w.shape[1] // narrow, step, 0)
-
-    def second(turn):
+        blocks = gate_w.shape[1] // narrow
+        lax.fori_loop(begin * blocks // CHUNKS, end * blocks // CHUNKS, step, 0)
+
+    def second(turn, begin, end):
         def step(number, carry):
             part[turn, :, cols(number)] = jnp.dot(
                 hidden[...], down_w[:, cols(number)], preferred_element_type=jnp.float32
@@ -201,9 +211,9 @@
             share_copy(turn, number).start()
             return carry
 
-        lax.fori_loop(0, CHUNKS, step, 0)
-
-    def third(turn):
+        lax.fori_loop(begin, end, step, 0)
+
+    def third(turn, begin, end):
         def step(number, carry):
             share_copy(turn, number).wait_recv()
             total = (
@@ -216,23 +226,20 @@
                 back_copy(turn, number, place).start()
             return carry
 
-        lax.fori_loop(0, CHUNKS, step, 0)
+        lax.fori_loop(begin, end, step, 0)
 
     def combined(turn, number):
-        for place in range(1, chips):
-            back_copy(turn, number, place).wait_recv()
+        back_copy(turn, number, 1, chips - 1).wait_recv()
         block = ret[turn, :, cols(number)]
         return jnp.dot(
             weights[flips[turn], 0], block, preferred_element_type=jnp.float32
         ) + jnp.dot(weights[flips[turn], 1], block, preferred_element_type=jnp.float32)
 
-    def end_chain(turn):
-        def step(number, carry):
+    def end_chain(turn, number):
+        @pl.when(is_end)
+        def _():
             zout[turn, :, cols(number)] = combined(turn, number).astype(jnp.bfloat16)
             chain_copy(turn, number).start()
-            return carry
-
-        lax.fori_loop(0, CHUNKS, step, 0)
 
     def mid_link(turn, number):
         partial = combined(turn, number)
@@ -242,65 +249,35 @@
         ).astype(jnp.bfloat16)
         chain_copy(turn, number).start()
 
-    def at_mid(turn, begin, end):
-        @pl.when(is_mid)
-        def _():
-            for number in range(begin, end):
-                arrive(turn, number, True)
-
-    def at_end(turn, begin, end):
-        @pl.when(is_end)
-        def _():
-            for number in range(begin, end):
-                arrive(turn, number, False)
-
-    def near(begin, end):
-        for number in range(begin, end):
-            at_mid(1, number, number + 1)
-            at_mid(2, number, number + 1)
-            at_end(1, number, number + 1)
-
+    def run(*steps):
+        for step, *rest in steps:
+            step(*rest)
+
+    G, F, U, T, C = gather, first, second, third, end_chain
+    A, B, E = near, next_near, far
     for number in range(CHUNKS):
-        select(0, number)
-    near(0, CHUNKS // 2)
-    gather(0)
-    first(0)
-    near(CHUNKS // 2, CHUNKS)
-    second(0)
-    at_mid(3, 0, CHUNKS // 4)
-    at_end(2, 0, CHUNKS // 4)
-    gather(1)
-    first(1)
-    at_mid(3, CHUNKS // 4, CHUNKS // 2)
-    at_end(2, CHUNKS // 4, CHUNKS // 2)
-    second(1)
-    third(1)
-    at_mid(3, CHUNKS // 2, CHUNKS)
-    at_end(2, CHUNKS // 2, CHUNKS)
-    pl.when(is_end)(lambda: end_chain(1))
-    at_end(3, 0, CHUNKS // 4)
-    gather(2)
-    first(2)
-    at_end(3, CHUNKS // 4, CHUNKS // 2)
-    second(2)
-    third(2)
-    at_end(3, CHUNKS // 2, CHUNKS)
-    pl.when(is_end)(lambda: end_chain(2))
-    third(0)
-    gather(3)
-    first(3)
-    second(3)
-    third(3)
-    pl.when(is_end)(lambda: end_chain(3))
+        select(0, 0, own, number)
+    run((A, 0), (A, 1), (A, 2), (A, 3), (G, 0), (F, 0, 0, 8))
+    run((A, 4), (A, 5), (U, 0, 0, 4), (A, 6), (U, 0, 4, 8), (A, 7), (B, 0))
+    run((G, 1), (F, 1, 0, 4), (B, 1), (B, 2), (F, 1, 4, 8), (B, 3), (U, 1, 0, 4), (B, 4))
+    run((U, 1, 4, 8), (B, 5), (T, 1, 0, 4), (B, 6), (T, 1, 4, 6), (B, 7), (T, 1, 6, 8), (C, 1, 0))
+    run((E, 0), (C, 1, 1), (C, 1, 2), (E, 1), (C, 1, 3), (C, 1, 4), (G, 2), (F, 2, 0, 4), (E, 2))
+    run((E, 3), (C, 1, 5), (C, 1, 6), (C, 1, 7), (F, 2, 4, 8), (E, 4), (U, 2, 0, 4), (E, 5))
+    run((U, 2, 4, 8), (T, 2, 0, 2), (E, 6), (T, 2, 2, 4), (E, 7), (T, 2, 4, 8), (C, 2, 0), (C, 2, 1))
+    run((C, 2, 2), (C, 2, 3), (G, 3), (F, 3, 0, 4), (C, 2, 4), (C, 2, 5), (C, 2, 6), (C, 2, 7))
+    run((F, 3, 4, 8), (U, 3, 0, 4), (U, 3, 4, 8), (T, 3, 0, 8), (T, 0, 0, 8))
+    for number in range(CHUNKS):
+        end_chain(3, number)
 
     @pl.when(is_mid)
     def _():
         for number in range(CHUNKS):
             mid_link(2, number)
-        mid_link(3, 0)
-        for number in range(1, CHUNKS):
+        for number in range(CHUNKS):
             mid_link(3, number)
-            mid_link(1, number - 1)
+            if number > 1:
+                mid_link(1, number - 2)
+        mid_link(1, CHUNKS - 2)
         mid_link(1, CHUNKS - 1)
 
     def finish(number, carry):
@@ -316,26 +293,26 @@
 
     lax.fori_loop(0, CHUNKS, finish, 0)
 
-    def drain(number, carry):
-        pl.when(has_left)(lambda: dispatch(0, number, -1, 0).wait_send())
-        pl.when(has_right)(lambda: dispatch(0, number, 1, 1).wait_send())
-
-        @pl.when(is_mid)
-        def _():
-            for turn in range(1, PLANES):
-                dispatch(turn, number, -ways[turn], 0).wait_send()
-
-        for turn in range(PLANES):
-            pair_copy(turn, number).wait_send()
-            share_copy(turn, number).wait_send()
-            for place in range(1, chips):
-                plane_copy(turn, number, place).wait_send()
-                back_copy(turn, number, place).wait_send()
-            if turn:
-                chain_copy(turn, number).wait_send()
-        return carry
-
-    lax.fori_loop(0, CHUNKS, drain, 0)
+    def sent(block, semaphore):
+        return pltpu.make_async_remote_copy(
+            src_ref=block,
+            dst_ref=block,
+            send_sem=semaphore.at[0],
+            recv_sem=semaphore.at[0],
+            device_id={"tp": other},
+            device_id_type=MESH,
+        )
+
+    pl.when(has_left)(lambda: sent(own, disp_sent).wait_send())
+    pl.when(has_right)(lambda: sent(own, disp_sent.at[pl.ds(1, 1)]).wait_send())
+    pl.when(is_mid)(
+        lambda: sent(dense.at[pl.ds(0, PLANES - 1)], disp_sent.at[pl.ds(2, 1)]).wait_send()
+    )
+    sent(rows.at[:, pl.ds(0, half)], pair_sent).wait_send()
+    sent(given, part_sent).wait_send()
+    sent(pick.at[:, pl.ds(0, half - cap)], plane_sent).wait_send()
+    sent(ret.at[:, pl.ds(0, half - cap)], back_sent).wait_send()
+    sent(zout.at[pl.ds(1, PLANES - 1)], chain_sent).wait_send()
 
 
 def run_experts(own, picks, weights, expert_gate, expert_up, expert_down, count, cap):
@@ -365,12 +342,12 @@
             pltpu.VMEM((width, units), held),
             pltpu.VMEM((width, units), held),
             pltpu.VMEM((units, width), held),
-            dma(PLANES, CHUNKS, 2), dma(PLANES, CHUNKS),
-            dma(PLANES, CHUNKS, chips), dma(PLANES, CHUNKS, chips),
-            dma(PLANES, CHUNKS), dma(PLANES, CHUNKS),
-            dma(PLANES, CHUNKS), dma(PLANES, CHUNKS),
-            dma(PLANES, CHUNKS, chips), dma(PLANES, CHUNKS, chips),
-            dma(PLANES, CHUNKS), dma(PLANES + 1, CHUNKS),
+            dma(3), dma(PLANES, CHUNKS),
+            dma(1), dma(PLANES, CHUNKS),
+            dma(1), dma(PLANES),
+            dma(1), dma(PLANES, CHUNKS),
+            dma(1), dma(PLANES, CHUNKS),
+            dma(1), dma(PLANES + 1, CHUNKS),
             dma(3),
         ],
         compiler_params=pltpu.CompilerParams(

time: 153 us -> 141 us (0.922)
  Pallas kernels: 123 us -> 111 us
    pallas_call x1, Pallas kernels: 123 us -> 111 us  [run_experts(): pl.pallas_call(functools.partial(experts_kernel, count, cap), out_shape=j...]
where the time goes in v3:
time: 141 us
  Pallas kernels  111 us (79%)
  other arithmetic  14.5 us (10%)
  starting transfers between devices  9.56 us (7%)
  local copies, waits for them, and re-layouts  2.55 us (2%)
  waiting for transfers between devices  1.41 us (1%)
    pallas_call x1, Pallas kernels, run_experts(): pl.pallas_call(functools.partial(experts_kernel, count, cap), out_shape=j...  111 us
    ppermute x5, starting transfers between devices, swap(): lax.ppermute(value, axis, [(source, source ^ offset) for source in range(...  5.94 us
    reduce_sum x1, other arithmetic, on_device(): sums = jnp.stack([jnp.sum(mixed, 1), jnp.sum(mixed * mixed, 1)])  3.83 us
    ppermute x1, starting transfers between devices, from_behind(): lax.ppermute(value, axis, [(source, source + steps) for source in range(f...  3.62 us
  transfers between devices with their start and end apart: 6, of which 3 were waited for; matrix products, arithmetic and copies ran while one was open for 3% of the time, Pallas kernels for 0%

profile of v3, /device:TPU:0, one launch (start us, length us, event | category | flops | bytes accessed | tf_op | source)
XLA Modules:
  0.0 140.9 jit_solution(4073797049224726476)
XLA Ops:
  0.0 0.0 copy-start.2
  0.0 0.8 copy.48
  0.8 0.1 eq.381
  1.0 0.1 eq.377
  1.1 0.9 reduce-window.6
  2.0 0.2 slice_reduce_fusion
  2.3 0.1 fusion.42
  2.4 0.1 reshape.1692
  2.5 0.1 copy.51
  2.6 0.7 add_convert_fusion.2
  3.3 0.7 maximum_bitcast_fusion.4
  4.0 4.1 %collective-permute-start.4 = (f32[4,192]{1,0:T(4,128)S(1)}, f32[4,192]{1,0:T(4,128)S(1)}, u32[]{:S(2)}, u32[]{:S(2)}) collective-permute-start(f32[4,192]{1,0:T(4,128)S(1)} %maximum_bitcast_fusion.4), channel_id=1, source_target_pairs={{0,16},{2,18},{4,20},{6,22},{8,24},{10,26},{12,28},{14,30},{16,0},... | collective-permute-start | bytes 9224 | tf_op jit(solution)/shard_map/ppermute | solution.py:367
  8.1 1.6 %collective-permute-start.3 = (f32[4,192]{1,0:T(4,128)S(1)}, f32[4,192]{1,0:T(4,128)S(1)}, u32[]{:S(2)}, u32[]{:S(2)}) collective-permute-start(f32[4,192]{1,0:T(4,128)S(1)} %maximum_bitcast_fusion.4), channel_id=1, source_target_pairs={{0,8},{2,10},{4,12},{6,14},{8,0},{10,2},{12,4},{14,6},{16,24},{18,... | collective-permute-start | bytes 9224 | tf_op jit(solution)/shard_map/ppermute | solution.py:367
  9.6 0.0 collective-permute-start.5
  9.6 1.3 multiply_convert_fusion.2
  11.0 3.6 %collective-permute-start = (bf16[30,512]{1,0:T(8,128)(2,1)S(1)}, bf16[30,512]{1,0:T(8,128)(2,1)S(1)}, u32[]{:S(2)}, u32[]{:S(2)}) collective-permute-start(bf16[30,512]{1,0:T(8,128)(2,1)S(1)} %slice.396), channel_id=1, source_target_pairs={{0,2},{2,4},{4,6},{6,8},{8,10},{10,12},{12,14},{14,16},{16,18},{18... | collective-permute-start | bytes 92168 | tf_op jit(solution)/shard_map/ppermute | solution.py:362
  14.6 0.0 copy-done.2
  14.7 0.0 copy-start.6
  14.8 0.0 collective-permute-done.4
  14.8 0.0 collective-permute-done.3
  14.8 0.2 collective-permute-done.5
  15.0 0.2 compare_or_fusion.3
  15.2 0.5 reduce-precision_convert_fusion.3
  15.7 0.8 add_convert_fusion.1.picks
  16.6 0.0 collective-permute-done
  16.6 0.1 maximum_convert_fusion
  16.7 0.0 copy-done.6
  16.7 0.0 copy-start.4
  16.7 0.0 copy-start.5
  16.7 3.8 %fusion.49 = (f32[384]{0:T(512)S(1)}, f32[384]{0:T(512)S(1)}, f32[384,512]{1,0:T(8,128)S(1)}) fusion(f32[414,512]{1,0:T(8,128)S(1)} %maximum_convert_fusion, f32[512]{0:T(512)S(1)} %bitcast.105, f32[512]{0:T(512)S(1)} %bitcast.106, f32[512]{0:T(512)S(1)} %bitcast.108, f32[512]{0:T(512)S(1)} %bitcast.109, f32[512]{0:T(512)S(1)} %bitcast.110, ...), kind=kLoop, calls=%fused_computation.132 | loop fusion | flops 12778752 | bytes 25234432 | tf_op jit(solution)/shard_map/reduce_sum | solution.py:401
  20.6 0.1 collective-permute-start.1
  20.7 0.1 maximum_bitcast_fusion
  20.8 1.1 collective-permute-done.1
  21.9 0.0 copy-done.4
  21.9 0.0 copy-done.5
  21.9 0.0 copy-start
  21.9 0.4 multiply_convert_fusion.1
  22.3 0.2 collective-permute-start.2
  22.5 0.0 copy-start.1
  22.5 0.1 maximum_bitcast_fusion.2
  22.6 1.1 pad_maximum_fusion.weights
  23.7 0.1 collective-permute-done.2
  23.9 0.5 copy-done
  24.4 0.4 copy-done.1
  24.7 0.0 copy-start.3
  24.7 1.1 multiply_reduce_fusion
  25.9 0.0 copy-done.3
  25.9 1.1 multiply_convert_fusion.own
  27.0 111.4 %shard_map.136 = f32[192,2048]{1,0:T(8,128)} custom-call(bf16[192,2048]{1,0:T(8,128)(2,1)} %multiply_convert_fusion.own, bf16[4,192,192]{2,1,0:T(8,128)(2,1)} %add_convert_fusion.1.picks, bf16[4,2,192,192]{3,2,1,0:T(8,128)(2,1)} %pad_maximum_fusion.weights, bf16[1,2048,1024]{2,1,0:T(8,128)(2,1)} %gate_in.1, bf16[1,2048,1024]{2,1,0:T(8,128)(2,1)} %up_in.1, ...), custom_call_target="tpu_custom_call" | custom-call | tf_op jit(solution)/shard_map/pallas_call | solution.py:327
  138.4 2.5 %add_convert_fusion = bf16[192,2048]{1,0:T(8,128)(2,1)} fusion(f32[192,2048]{1,0:T(8,128)S(1)} %get-tuple-element.78, f32[192,2048]{1,0:T(8,128)} %shard_map.136), kind=kLoop, calls=%fused_computation.3 | loop fusion | flops 786432 | bytes 3932160 | tf_op jit(solution)/shard_map/convert_element_type | solution.py:462
  (19 shorter events, 0.3 us)
Async XLA Ops:
  0.0 14.6 %copy-start.2 = (f32[31,512]{1,0:T(8,128)S(1)}, f32[31,512]{1,0:T(8,128)}, u32[]{:S(2)}) copy-start(f32[31,512]{1,0:T(8,128)} %param.17) | copy-start | bytes 190468
  4.0 10.8 %collective-permute-start.4 = (f32[4,192]{1,0:T(4,128)S(1)}, f32[4,192]{1,0:T(4,128)S(1)}, u32[]{:S(2)}, u32[]{:S(2)}) collective-permute-start(f32[4,192]{1,0:T(4,128)S(1)} %maximum_bitcast_fusion.4), channel_id=1, source_target_pairs={{0,16},{2,18},{4,20},{6,22},{8,24},{10,26},{12,28},{14,30},{16,0},... | collective-permute-start | bytes 9224 | tf_op jit(solution)/shard_map/ppermute | solution.py:367
  8.1 6.7 %collective-permute-start.3 = (f32[4,192]{1,0:T(4,128)S(1)}, f32[4,192]{1,0:T(4,128)S(1)}, u32[]{:S(2)}, u32[]{:S(2)}) collective-permute-start(f32[4,192]{1,0:T(4,128)S(1)} %maximum_bitcast_fusion.4), channel_id=1, source_target_pairs={{0,8},{2,10},{4,12},{6,14},{8,0},{10,2},{12,4},{14,6},{16,24},{18,... | collective-permute-start | bytes 9224 | tf_op jit(solution)/shard_map/ppermute | solution.py:367
  9.6 5.4 %collective-permute-start.5 = (f32[4,192]{1,0:T(4,128)S(1)}, f32[4,192]{1,0:T(4,128)S(1)}, u32[]{:S(2)}, u32[]{:S(2)}) collective-permute-start(f32[4,192]{1,0:T(4,128)S(1)} %maximum_bitcast_fusion.4), channel_id=1, source_target_pairs={{0,24},{2,26},{4,28},{6,30},{8,16},{10,18},{12,20},{14,22},{16,8},... | collective-permute-start | bytes 9224 | tf_op jit(solution)/shard_map/ppermute | solution.py:367
  11.0 5.6 %collective-permute-start = (bf16[30,512]{1,0:T(8,128)(2,1)S(1)}, bf16[30,512]{1,0:T(8,128)(2,1)S(1)}, u32[]{:S(2)}, u32[]{:S(2)}) collective-permute-start(bf16[30,512]{1,0:T(8,128)(2,1)S(1)} %slice.396), channel_id=1, source_target_pairs={{0,2},{2,4},{4,6},{6,8},{8,10},{10,12},{12,14},{14,16},{16,18},{18... | collective-permute-start | bytes 92168 | tf_op jit(solution)/shard_map/ppermute | solution.py:362
  14.7 2.0 %copy-start.6 = (f32[512]{0:T(512)S(1)}, f32[512]{0:T(512)}, u32[]{:S(2)}) copy-start(f32[512]{0:T(512)} %param.18) | copy-start | bytes 6148
  16.7 5.2 %copy-start.4 = (f32[512]{0:T(512)S(1)}, f32[512]{0:T(512)}, u32[]{:S(2)}) copy-start(f32[512]{0:T(512)} %param.20) | copy-start | bytes 6148
  16.7 5.2 %copy-start.5 = (f32[512]{0:T(512)S(1)}, f32[512]{0:T(512)}, u32[]{:S(2)}) copy-start(f32[512]{0:T(512)} %param.19) | copy-start | bytes 6148
  20.6 1.2 collective-permute-start.1
  21.9 2.5 %copy-start = (bf16[1024,2048]{1,0:T(8,128)(2,1)S(1)}, bf16[1024,2048]{1,0:T(8,128)(2,1)}, u32[]{:S(2)}) copy-start(bf16[1024,2048]{1,0:T(8,128)(2,1)} %param.21) | copy-start | bytes 12582916
  22.3 1.5 %collective-permute-start.2 = (bf16[192,512]{1,0:T(8,128)(2,1)S(1)}, bf16[192,512]{1,0:T(8,128)(2,1)S(1)}, u32[]{:S(2)}, u32[]{:S(2)}) collective-permute-start(bf16[192,512]{1,0:T(8,128)(2,1)S(1)} %broadcast_select_fusion.2), channel_id=1, source_target_pairs={{0,1},{1,0},{2,3},{3,2},{4,5},{5,4},{6,7},{7,6},{8,9},{9,8},{10,11... | collective-permute-start | bytes 589832 | tf_op jit(solution)/shard_map/ppermute | solution.py:367
  22.5 2.2 %copy-start.1 = (bf16[192,2048]{1,0:T(8,128)(2,1)S(1)}, bf16[192,2048]{1,0:T(8,128)(2,1)}, u32[]{:S(2)}) copy-start(bf16[192,2048]{1,0:T(8,128)(2,1)} %param.14) | copy-start | bytes 2359300
  24.7 1.2 copy-start.3

commit v4 on v3

--- a/solution.py
+++ b/solution.py
@@ -21,13 +21,21 @@
     return result
 
 
-def experts_kernel(
-    count, cap, own, picks, weights, gate_in, up_in, down_in, out,
+def layer_kernel(
+    count, cap, values, gates, taps, bias, gain, shift, norm_gain, ids, scales,
+    residual_in, mix_in, gate_in, up_in, down_in, out,
     dense, pick, rows, part, given, hidden, ret, zout, zin, gate_w, up_w, down_w,
+    extended, mixed, tail, stats, swapped, acted, route, picks, weights,
     disp_sent, disp_came, plane_sent, plane_came, pair_sent, pair_came, part_sent, part_came,
-    back_sent, back_came, chain_sent, chain_came, loaded,
+    back_sent, back_came, chain_sent, chain_came, loaded, mix_sent, mix_came,
 ):
-    me, other = lax.axis_index("sp"), 1 - lax.axis_index("tp")
+    me, core = lax.axis_index("sp"), lax.axis_index("tp")
+    other = 1 - core
+    row_count, width = dense.shape[1], dense.shape[2]
+    tok_count, chan = values.shape
+    taps_count, groups = taps.shape[0], chan // 128
+    pad = extended.shape[1] - tok_count
+    after = zout.at[0]
     chips = count // PLANES
     half = chips * cap
     z = me // chips
@@ -46,7 +54,8 @@
     crossed = (z, z + 1 - 2 * (z % 2), z + 2 - 4 * low, PLANES - 1 - z)
     aways = (0, 2 * (z % 2) - 1, 2 * low - 1, 2 * low - 1)
     has_left, has_right = z > 0, z < PLANES - 1
-    wide = own.shape[1] // CHUNKS
+    wide = width // CHUNKS
+    own = dense.at[z]
 
     def cols(number):
         return pl.ds(pl.multiple_of(number * wide, wide), wide)
@@ -120,12 +129,17 @@
         )
 
     loads = [
-        pltpu.make_async_copy(source.at[0], target, loaded.at[number])
+        pltpu.make_async_copy(source, target, loaded.at[number])
         for number, (source, target) in enumerate(
-            ((gate_in, gate_w), (up_in, up_w), (down_in, down_w))
+            (
+                (gate_in.at[0], gate_w), (up_in.at[0], up_w), (down_in.at[0], down_w),
+                (mix_in, down_w), (residual_in, after),
+            )
         )
     ]
-    for load in loads:
+    early = loads[3:]
+    loads = loads[:3]
+    for load in early + loads[:2]:
         load.start()
 
     barrier = pltpu.get_barrier_semaphore()
@@ -135,22 +149,187 @@
         )
     pl.semaphore_signal(barrier, inc=1, device_id={"tp": other}, device_id_type=MESH)
 
-    @pl.when(has_left)
+    for flip in range(1, PLANES):
+        pl.semaphore_signal(
+            barrier, inc=1, device_id={"sp": crossed[flip] * chips + me % chips}, device_id_type=MESH
+        )
+
+    def greet(step):
+        pl.semaphore_signal(barrier, inc=1, device_id={"sp": me + step}, device_id_type=MESH)
+
+    not_first, not_last = me > 0, me < count - 1
+    pl.when(not_first)(lambda: greet(-1))
+    pl.when(not_last)(lambda: greet(1))
+
+    def gated(first_row, row_total, lanes):
+        chosen = (pl.ds(first_row, row_total), lanes)
+        return (
+            values[chosen].astype(jnp.float32) * jax.nn.sigmoid(gates[chosen].astype(jnp.float32))
+        ).astype(jnp.bfloat16)
+
+    tail[0] = gated(tok_count - pad, pad, pl.ds(0, chan))
+    pl.semaphore_wait(
+        barrier,
+        chips + PLANES - 1 + (me + count - 2) // (count - 1) + (2 * count - 3 - me) // (count - 1),
+    )
+
+    def mix_copy(source, target, number, device):
+        return pltpu.make_async_remote_copy(
+            src_ref=source,
+            dst_ref=target,
+            send_sem=mix_sent.at[number],
+            recv_sem=mix_came.at[number],
+            device_id=device,
+            device_id_type=MESH,
+        )
+
+    halo = mix_copy(tail.at[0], tail.at[1], 0, {"sp": me + 1})
+    moments = mix_copy(stats.at[0], stats.at[1], 1, {"tp": other})
+    mine = pl.ds(pl.multiple_of(core * chan, chan), chan)
+    exchange = mix_copy(swapped, acted.at[:, mine], 2, {"tp": other})
+    routings = [
+        mix_copy(
+            route.at[0], route.at[flip], 2 + flip, {"sp": crossed[flip] * chips + me % chips}
+        )
+        for flip in range(1, PLANES)
+    ]
+    pl.when(not_last)(lambda: halo.start())
+
+    experts_all = count
+    expert_rows = lax.broadcasted_iota(jnp.int32, (experts_all, row_count), 0)
+    named = [expert_rows == ids[choice : choice + 1, :] for choice in range(ids.shape[0])]
+    onehot = sum(jnp.where(match, 1.0, 0.0) for match in named).astype(jnp.bfloat16)
+    earlier = jnp.where(
+        lax.broadcasted_iota(jnp.int32, (row_count, row_count), 0)
+        < lax.broadcasted_iota(jnp.int32, (row_count, row_count), 1),
+        1.0,
+        0.0,
+    ).astype(jnp.bfloat16)
+    before = jnp.dot(onehot, earlier, preferred_element_type=jnp.float32)
+    places = (
+        (expert_rows // chips) * half
+        + ((expert_rows % chips) ^ (me % chips)) * cap
+    ).astype(jnp.float32) + before
+    for choice, match in enumerate(named):
+        route[0, choice : choice + 1, :] = jnp.sum(
+            jnp.where(match, places, 0.0), 0, keepdims=True
+        )
+    lowest = ids.shape[0]
+    route[0, lowest : 2 * lowest, :] = scales[...]
+    for copy in routings:
+        copy.start()
+
+    for group in range(groups):
+        extended[group, pl.ds(pad, tok_count), :] = gated(
+            0, tok_count, pl.ds(group * 128, 128)
+        ).astype(jnp.float32)
+
+    @pl.when(not_first)
     def _():
-        pl.semaphore_signal(barrier, inc=1, device_id=along(-1), device_id_type=MESH)
-
-    @pl.when(has_right)
+        halo.wait_recv()
+        for group in range(groups):
+            extended[group, pl.ds(0, pad), :] = tail[1, :, pl.ds(group * 128, 128)].astype(
+                jnp.float32
+            )
+
+    @pl.when(me == 0)
     def _():
-        pl.semaphore_signal(barrier, inc=1, device_id=along(1), device_id_type=MESH)
-
-    pl.semaphore_wait(barrier, chips + (z + 2) // 3 + (PLANES + 1 - z) // 3)
+        extended[:, pl.ds(0, pad), :] = jnp.zeros((groups, pad, 128), jnp.float32)
+
+    block_rows = 64
+
+    def convolve(number, carry):
+        start = pl.multiple_of(number * block_rows, block_rows)
+        total = jnp.zeros((block_rows, 128), jnp.float32)
+        squares = total
+        for group in range(groups):
+            lanes = pl.ds(group * 128, 128)
+            result = jnp.broadcast_to(bias[:, lanes], (block_rows, 128))
+            for tap in range(taps_count):
+                result = result + taps[tap : tap + 1, lanes] * (
+                    extended[group, pl.ds(start + pad - taps_count + 1 + tap, block_rows), :]
+                )
+            mixed[group, pl.ds(start, block_rows), :] = result
+            total = total + result
+            squares = squares + result * result
+        left = lax.broadcasted_iota(jnp.int32, (block_rows, 128), 1) < 64
+        stats[0, pl.ds(start, block_rows), :] = jnp.where(
+            left, jnp.sum(total, 1, keepdims=True), jnp.sum(squares, 1, keepdims=True)
+        )
+        return carry
+
+    lax.fori_loop(0, tok_count // block_rows, convolve, 0)
+    moments.start()
+    def clear(landing):
+        zin[landing] = jnp.zeros((row_count, width), jnp.bfloat16)
+
+    pl.when(jnp.logical_not(has_left))(lambda: clear(z))
+    pl.when(jnp.logical_not(has_right))(lambda: clear(PLANES))
+    moments.wait_recv()
+
+    def activate(half_index, store):
+        start = pl.multiple_of(half_index * row_count, row_count)
+        both = stats[0, pl.ds(start, row_count), :] + stats[1, pl.ds(start, row_count), :]
+        center = both[:, 0:1] / (2 * chan)
+        scale = lax.rsqrt(both[:, 64:65] / (2 * chan) - center * center + 1e-06)
+        for group in range(groups):
+            lanes = pl.ds(group * 128, 128)
+            normed = (mixed[group, pl.ds(start, row_count), :] - center) * scale * gain[
+                :, lanes
+            ] + shift[:, lanes]
+            store(group, jax.nn.silu(normed).astype(jnp.bfloat16))
+
+    def store_swapped(group, value):
+        swapped[:, pl.ds(group * 128, 128)] = value
+
+    def store_mine(group, value):
+        acted[:, pl.ds(pl.multiple_of(core * chan + group * 128, 128), 128)] = value
+
+    activate(other, store_swapped)
+    exchange.start()
+    activate(core, store_mine)
+    for load in early:
+        load.wait()
+    exchange.wait_recv()
+
+    def project(number, carry):
+        block = (
+            after[:, cols(number)].astype(jnp.float32)
+            + jnp.dot(acted[...], down_w[:, cols(number)], preferred_element_type=jnp.float32)
+        ).astype(jnp.bfloat16)
+        after[:, cols(number)] = block
+        wider = block.astype(jnp.float32)
+        return carry + jnp.sum(wider * wider, 1, keepdims=True)
+
+    power = lax.fori_loop(0, CHUNKS, project, jnp.zeros((row_count, 1), jnp.float32))
+    loads[2].start()
+    level = lax.rsqrt(power / width + 1e-06)
 
     def send_own(number, carry):
-        pl.when(has_left)(lambda: dispatch(z, number, -1, 0, own).start())
-        pl.when(has_right)(lambda: dispatch(z, number, 1, 1, own).start())
+        own[:, cols(number)] = (
+            after[:, cols(number)].astype(jnp.float32) * level * norm_gain[:, cols(number)]
+        ).astype(jnp.bfloat16)
+        pl.when(has_left)(lambda: dispatch(z, number, -1, 0).start())
+        pl.when(has_right)(lambda: dispatch(z, number, 1, 1).start())
         return carry
 
     lax.fori_loop(0, CHUNKS, send_own, 0)
+
+    def place(flip):
+        slots = (
+            lax.broadcasted_iota(jnp.int32, (half, row_count), 0) + z * half
+        ).astype(jnp.float32)
+        matches = [slots == route[flip, choice : choice + 1, :] for choice in range(lowest)]
+        picks[flip] = sum(jnp.where(match, 1.0, 0.0) for match in matches).astype(jnp.bfloat16)
+        weighting = sum(
+            jnp.where(match, route[flip, lowest + choice : lowest + choice + 1, :], 0.0)
+            for choice, match in enumerate(matches)
+        )
+        coarse = weighting.astype(jnp.bfloat16)
+        weights[flip, 0] = coarse
+        weights[flip, 1] = (weighting - coarse.astype(jnp.float32)).astype(jnp.bfloat16)
+
+    place(0)
 
     def select(turn, flip, block, number):
         chosen = jnp.dot(
@@ -231,9 +410,12 @@
     def combined(turn, number):
         back_copy(turn, number, 1, chips - 1).wait_recv()
         block = ret[turn, :, cols(number)]
-        return jnp.dot(
-            weights[flips[turn], 0], block, preferred_element_type=jnp.float32
-        ) + jnp.dot(weights[flips[turn], 1], block, preferred_element_type=jnp.float32)
+        across = (((0,), (0,)), ((), ()))
+        return lax.dot_general(
+            weights[flips[turn], 0], block, across, preferred_element_type=jnp.float32
+        ) + lax.dot_general(
+            weights[flips[turn], 1], block, across, preferred_element_type=jnp.float32
+        )
 
     def end_chain(turn, number):
         @pl.when(is_end)
@@ -257,6 +439,9 @@
     A, B, E = near, next_near, far
     for number in range(CHUNKS):
         select(0, 0, own, number)
+    for flip in range(1, PLANES):
+        routings[flip - 1].wait_recv()
+        place(flip)
     run((A, 0), (A, 1), (A, 2), (A, 3), (G, 0), (F, 0, 0, 8))
     run((A, 4), (A, 5), (U, 0, 0, 4), (A, 6), (U, 0, 4, 8), (A, 7), (B, 0))
     run((G, 1), (F, 1, 0, 4), (B, 1), (B, 2), (F, 1, 4, 8), (B, 3), (U, 1, 0, 4), (B, 4))
@@ -281,14 +466,14 @@
         mid_link(1, CHUNKS - 1)
 
     def finish(number, carry):
-        out[:, cols(number)] = combined(0, number)
-
-        def joined(landing):
-            chain_copy(1, number, landing).wait_recv()
-            out[:, cols(number)] += zin[landing, :, cols(number)].astype(jnp.float32)
-
-        pl.when(has_left)(lambda: joined(z))
-        pl.when(has_right)(lambda: joined(PLANES))
+        total = after[:, cols(number)].astype(jnp.float32) + combined(0, number)
+        pl.when(has_left)(lambda: chain_copy(1, number, z).wait_recv())
+        pl.when(has_right)(lambda: chain_copy(1, number, PLANES).wait_recv())
+        out[:, cols(number)] = (
+            total
+            + zin[z, :, cols(number)].astype(jnp.float32)
+            + zin[PLANES, :, cols(number)].astype(jnp.float32)
+        ).astype(jnp.bfloat16)
         return carry
 
     lax.fori_loop(0, CHUNKS, finish, 0)
@@ -303,6 +488,11 @@
             device_id_type=MESH,
         )
 
+    pl.when(not_last)(lambda: halo.wait_send())
+    moments.wait_send()
+    exchange.wait_send()
+    for copy in routings:
+        copy.wait_send()
     pl.when(has_left)(lambda: sent(own, disp_sent).wait_send())
     pl.when(has_right)(lambda: sent(own, disp_sent.at[pl.ds(1, 1)]).wait_send())
     pl.when(is_mid)(
@@ -315,19 +505,26 @@
     sent(zout.at[pl.ds(1, PLANES - 1)], chain_sent).wait_send()
 
 
-def run_experts(own, picks, weights, expert_gate, expert_up, expert_down, count, cap):
-    row_count, width = own.shape
+def run_layer(
+    values, gates, taps, bias, gain, shift, norm_gain, ids, scales,
+    residual_in, out_weight, expert_gate, expert_up, expert_down, count, cap,
+):
+    row_count, width = residual_in.shape
+    tok_count, chan = values.shape
     units = expert_gate.shape[2]
     chips = count // PLANES
     half = chips * cap
+    pad = (taps.shape[0] + 14) // 16 * 16
+    groups = chan // 128
+    choose_count = ids.shape[0]
     dma = lambda *shape: pltpu.SemaphoreType.DMA(shape)
     vmem = pl.BlockSpec(memory_space=pltpu.VMEM)
     anywhere = pl.BlockSpec(memory_space=pl.ANY)
     held = jnp.bfloat16
     return pl.pallas_call(
-        functools.partial(experts_kernel, count, cap),
-        out_shape=jax.ShapeDtypeStruct((row_count, width), jnp.float32),
-        in_specs=[vmem, vmem, vmem, anywhere, anywhere, anywhere],
+        functools.partial(layer_kernel, count, cap),
+        out_shape=jax.ShapeDtypeStruct((row_count, width), held),
+        in_specs=[vmem] * 9 + [anywhere] * 5,
         out_specs=vmem,
         scratch_shapes=[
             pltpu.VMEM((PLANES, row_count, width), held),
@@ -342,29 +539,30 @@
             pltpu.VMEM((width, units), held),
             pltpu.VMEM((width, units), held),
             pltpu.VMEM((units, width), held),
+            pltpu.VMEM((groups, pad + tok_count, 128), jnp.float32),
+            pltpu.VMEM((groups, tok_count, 128), jnp.float32),
+            pltpu.VMEM((2, pad, chan), held),
+            pltpu.VMEM((2, tok_count, 128), jnp.float32),
+            pltpu.VMEM((row_count, chan), held),
+            pltpu.VMEM((row_count, 2 * chan), held),
+            pltpu.VMEM((PLANES, 2 * choose_count, row_count), jnp.float32),
+            pltpu.VMEM((PLANES, half, row_count), held),
+            pltpu.VMEM((PLANES, 2, half, row_count), held),
             dma(3), dma(PLANES, CHUNKS),
             dma(1), dma(PLANES, CHUNKS),
             dma(1), dma(PLANES),
             dma(1), dma(PLANES, CHUNKS),
             dma(1), dma(PLANES, CHUNKS),
             dma(1), dma(PLANES + 1, CHUNKS),
-            dma(3),
+            dma(5), dma(2 + PLANES), dma(2 + PLANES),
         ],
         compiler_params=pltpu.CompilerParams(
-            collective_id=0, has_side_effects=True, vmem_limit_bytes=62 * 1024 * 1024
+            collective_id=0, has_side_effects=True, vmem_limit_bytes=63 * 1024 * 1024
         ),
-    )(own, picks, weights, expert_gate, expert_up, expert_down)
-
-
-def from_behind(value, axis, steps):
-    count = lax.axis_size(axis)
-    first, last = (max(0, -steps), min(count, count - steps))
-    return lax.ppermute(value, axis, [(source, source + steps) for source in range(first, last)])
-
-
-def swap(value, axis, offset):
-    count = lax.axis_size(axis)
-    return lax.ppermute(value, axis, [(source, source ^ offset) for source in range(count)])
+    )(
+        values, gates, taps, bias, gain, shift, norm_gain, ids, scales,
+        residual_in, out_weight, expert_gate, expert_up, expert_down,
+    )
 
 
 def on_device(
@@ -383,83 +581,29 @@
     expert_up,
     expert_down,
 ):
-    taps_count = conv_kernel.shape[0]
-    tok_count, local_chan = conv_values.shape
-    tp_count = lax.axis_size("tp")
-    all_chan = local_chan * tp_count
-    core = lax.axis_index("tp")
-    gated = (
-        conv_values.astype(jnp.float32) * jax.nn.sigmoid(conv_gates.astype(jnp.float32))
-    ).astype(jnp.bfloat16)
-    earlier = from_behind(gated[tok_count - (taps_count - 1) :], "sp", 1)
-    extended = jnp.concatenate([earlier, gated], 0).astype(jnp.float32)
-    mixed = jnp.zeros((tok_count, local_chan), jnp.float32) + conv_bias[None, :]
-    for tap_index in range(taps_count):
-        mixed = (
-            mixed + conv_kernel[tap_index][None, :] * extended[tap_index : tap_index + tok_count]
-        )
-    sums = jnp.stack([jnp.sum(mixed, 1), jnp.sum(mixed * mixed, 1)])
-    sums = sums + swap(sums, "tp", 1)
-    center = (sums[0] / all_chan)[:, None]
-    spread = (sums[1] / all_chan)[:, None] - center * center
-    normed = (mixed - center) * lax.rsqrt(spread + 1e-06) * chan_gain[None, :] + chan_shift[None, :]
-    activated = jax.nn.silu(normed).astype(jnp.bfloat16)
-    row_count = tok_count // tp_count
-    low, high = activated[:row_count], activated[row_count:]
-    kept = jnp.where(core == 0, low, high)
-    given = swap(jnp.where(core == 0, high, low), "tp", 1)
-    regrouped = jnp.concatenate(
-        [jnp.where(core == 0, kept, given), jnp.where(core == 0, given, kept)], 1
-    )
-    projected = jnp.dot(regrouped, out_weight, preferred_element_type=jnp.float32)
-    after_f = (residual_in.astype(jnp.float32) + projected).astype(jnp.bfloat16).astype(jnp.float32)
-    normal_rows = (
-        after_f
-        * lax.rsqrt(jnp.mean(after_f * after_f, 1, keepdims=True) + 1e-06)
-        * norm_gain[None, :]
-    ).astype(jnp.bfloat16)
     sp_count = lax.axis_size("sp")
     experts_all = expert_gate.shape[0] * sp_count
-    choose_count = route_ids.shape[1]
+    choose_count, row_count = route_ids.shape[1], residual_in.shape[0]
     slot_cap = max(2, (2 * choose_count * row_count + experts_all - 1) // experts_all)
     slot_cap = (slot_cap + 15) // 16 * 16
-    onehot = (
-        route_ids.reshape(-1)[:, None] == jnp.arange(experts_all, dtype=jnp.int32)[None, :]
-    ).astype(jnp.int32)
-    before = jnp.cumsum(onehot, 0) - onehot
-    ranking = jnp.sum(before * onehot, 1).reshape(row_count, choose_count)
-    chips = sp_count // PLANES
-    half = chips * slot_cap
-    me = lax.axis_index("sp")
-    plane, place = me // chips, me % chips
-    target_plane, target_place = route_ids // chips, route_ids % chips
-    slot_ids = target_plane * half + (target_place ^ place) * slot_cap + ranking
-    routing = jnp.concatenate([slot_ids.astype(jnp.float32), route_weights], 1).T
-    routings = [routing] + [swap(routing, "sp", flip * chips) for flip in range(1, PLANES)]
-    base = (plane * half).astype(jnp.float32)
-    slots = lax.broadcasted_iota(jnp.int32, (half, 1), 0).astype(jnp.float32) + base
-    lanes = lax.broadcasted_iota(jnp.int32, (1, half), 1).astype(jnp.float32) + base
-    picks, weights = [], []
-    for held in routings:
-        ids, scales = held[:choose_count], held[choose_count:]
-        chosen = functools.reduce(
-            jnp.logical_or, [slots == ids[choice][None, :] for choice in range(choose_count)]
-        )
-        picks.append(chosen.astype(jnp.bfloat16))
-        weighting = sum(
-            jnp.where(lanes == ids[choice][:, None], scales[choice][:, None], 0.0)
-            for choice in range(choose_count)
-        )
-        coarse_f = lax.reduce_precision(weighting, 8, 7)
-        weights.append(
-            jnp.stack([coarse_f.astype(jnp.bfloat16), (weighting - coarse_f).astype(jnp.bfloat16)])
-        )
-    summed = run_experts(
-        normal_rows, jnp.stack(picks), jnp.stack(weights),
-        expert_gate, expert_up, expert_down, sp_count, slot_cap,
+    return run_layer(
+        conv_values,
+        conv_gates,
+        conv_kernel,
+        conv_bias[None, :],
+        chan_gain[None, :],
+        chan_shift[None, :],
+        norm_gain[None, :],
+        route_ids.T,
+        route_weights.T,
+        residual_in,
+        out_weight,
+        expert_gate,
+        expert_up,
+        expert_down,
+        sp_count,
+        slot_cap,
     )
-    combined = after_f + summed
-    return combined.astype(jnp.bfloat16)
 
 
 def solution(mesh):

time: 141 us -> 128 us (0.908)
  Pallas kernels: 111 us -> 126 us
  other arithmetic: 14.5 us -> 0 us
  starting transfers between devices: 9.56 us -> 0 us
  waiting for transfers between devices: 1.41 us -> 0 us
    pallas_call x1, Pallas kernels: 111 us -> 126 us  [run_layer(): pl.pallas_call(functools.partial(layer_kernel, count, cap), out_shape=jax...]
    ppermute x6 -> x0, starting transfers between devices: 9.56 us -> none  [the longest x5 5.94 us: swap(): lax.ppermute(value, axis, [(source, source ^ offset) for source in range(...]
    convert_element_type x8 -> x0, other arithmetic: 6.57 us -> none  [the longest x1 2.48 us: on_device(): return combined.astype(jnp.bfloat16)]
    reduce_sum x2 -> x0, other arithmetic: 3.93 us -> none  [the longest x1 3.83 us: on_device(): sums = jnp.stack([jnp.sum(mixed, 1), jnp.sum(mixed * mixed, 1)])]
    another operation x7 -> x0, other arithmetic: 2.98 us -> none  [the longest x3 1.23 us: on_device(): jnp.stack(weights)]
    ppermute x6 -> x0, waiting for transfers between devices: 1.41 us -> none  [the longest x5 1.41 us: swap(): lax.ppermute(value, axis, [(source, source ^ offset) for source in range(...]
  transfers between devices with their start and end apart: 6 -> 0, of which waited for: 3 -> 0; matrix products, arithmetic and copies ran while one was open for 3% -> 0% of each run, Pallas kernels for 0% -> 0%
where the time goes in v4:
time: 128 us
  Pallas kernels  126 us (98%)
  local copies, waits for them, and re-layouts  2.09 us (2%)
    pallas_call x1, Pallas kernels, run_layer(): pl.pallas_call(functools.partial(layer_kernel, count, cap), out_shape=jax...  126 us

profile of v4, /device:TPU:0, one launch (start us, length us, event | category | flops | bytes accessed | tf_op | source)
XLA Modules:
  0.0 127.6 jit_solution(7386800713935921470)
XLA Ops:
  0.0 125.5 %shard_map.136 = bf16[192,2048]{1,0:T(8,128)(2,1)} custom-call(bf16[384,512]{1,0:T(8,128)(2,1)} %values.1, bf16[384,512]{1,0:T(8,128)(2,1)} %gates.1, f32[31,512]{1,0:T(8,128)} %taps.1, f32[1,512]{1,0:T(1,128)} %bitcast.7, f32[1,512]{1,0:T(1,128)} %bitcast.8, f32[1,512]{1,0:T(1,128)} %bitcast.9, f32[1,2048]{1,0:T(1,128)} %bitcast.6, s32[2,192]{1,0:T(2,128)} %bitcast.10, ...), custom_call_target="tpu_custom_call" | custom-call | tf_op jit(solution)/shard_map/pallas_call | solution.py:524
  125.5 2.1 %copy.16 = bf16[192,2048]{1,0:T(8,128)(2,1)} copy(bf16[192,2048]{1,0:T(8,128)(2,1)} %shard_map.136) | data formatting | bytes 1572864

commit v5 on v4

--- a/solution.py
+++ b/solution.py
@@ -41,15 +41,16 @@
     z = me // chips
     mid = ((z + 1) // 2) % 2
     low = z // 2
-    sources = (z, z + 1 - 2 * (z % 2), 2 - low, 3 * (1 - low))
-    flips = (0, 1, 2 + mid, 3 - mid)
+    sources = (z, z + 1 - 2 * (z % 2), 3 * (1 - low), 2 - low)
+    flips = (0, 1, 3 - mid, 2 + mid)
     ways = (0, 1 - 2 * (z % 2), 1 - 2 * low, 1 - 2 * low)
     landings = (
         0,
         sources[1] + (PLANES - sources[1]) * (z % 2),
-        sources[2] + (PLANES - sources[2]) * low * (1 - z % 2),
-        sources[3],
+        sources[2],
+        sources[3] + (PLANES - sources[3]) * low * (1 - z % 2),
     )
+    inner = 1 - 2 * low
     is_mid, is_end = mid == 1, mid == 0
     crossed = (z, z + 1 - 2 * (z % 2), z + 2 - 4 * low, PLANES - 1 - z)
     aways = (0, 2 * (z % 2) - 1, 2 * low - 1, 2 * low - 1)
@@ -59,6 +60,9 @@
 
     def cols(number):
         return pl.ds(pl.multiple_of(number * wide, wide), wide)
+
+    def pairs(number):
+        return pl.ds(pl.multiple_of(number * 2 * wide, 2 * wide), 2 * wide)
 
     def every(number):
         return pl.ds(0, CHUNKS * wide) if number is None else cols(number)
@@ -224,18 +228,6 @@
             0, tok_count, pl.ds(group * 128, 128)
         ).astype(jnp.float32)
 
-    @pl.when(not_first)
-    def _():
-        halo.wait_recv()
-        for group in range(groups):
-            extended[group, pl.ds(0, pad), :] = tail[1, :, pl.ds(group * 128, 128)].astype(
-                jnp.float32
-            )
-
-    @pl.when(me == 0)
-    def _():
-        extended[:, pl.ds(0, pad), :] = jnp.zeros((groups, pad, 128), jnp.float32)
-
     block_rows = 64
 
     def convolve(number, carry):
@@ -258,7 +250,21 @@
         )
         return carry
 
-    lax.fori_loop(0, tok_count // block_rows, convolve, 0)
+    lax.fori_loop(1, tok_count // block_rows, convolve, 0)
+
+    @pl.when(not_first)
+    def _():
+        halo.wait_recv()
+        for group in range(groups):
+            extended[group, pl.ds(0, pad), :] = tail[1, :, pl.ds(group * 128, 128)].astype(
+                jnp.float32
+            )
+
+    @pl.when(me == 0)
+    def _():
+        extended[:, pl.ds(0, pad), :] = jnp.zeros((groups, pad, 128), jnp.float32)
+
+    convolve(0, 0)
     moments.start()
     def clear(landing):
         zin[landing] = jnp.zeros((row_count, width), jnp.bfloat16)
@@ -294,14 +300,14 @@
 
     def project(number, carry):
         block = (
-            after[:, cols(number)].astype(jnp.float32)
-            + jnp.dot(acted[...], down_w[:, cols(number)], preferred_element_type=jnp.float32)
+            after[:, pairs(number)].astype(jnp.float32)
+            + jnp.dot(acted[...], down_w[:, pairs(number)], preferred_element_type=jnp.float32)
         ).astype(jnp.bfloat16)
-        after[:, cols(number)] = block
+        after[:, pairs(number)] = block
         wider = block.astype(jnp.float32)
         return carry + jnp.sum(wider * wider, 1, keepdims=True)
 
-    power = lax.fori_loop(0, CHUNKS, project, jnp.zeros((row_count, 1), jnp.float32))
+    power = lax.fori_loop(0, CHUNKS // 2, project, jnp.zeros((row_count, 1), jnp.float32))
     loads[2].start()
     level = lax.rsqrt(power / width + 1e-06)
 
@@ -309,11 +315,18 @@
         own[:, cols(number)] = (
             after[:, cols(number)].astype(jnp.float32) * level * norm_gain[:, cols(number)]
         ).astype(jnp.bfloat16)
-        pl.when(has_left)(lambda: dispatch(z, number, -1, 0).start())
-        pl.when(has_right)(lambda: dispatch(z, number, 1, 1).start())
+        pl.when(is_mid)(lambda: dispatch(z, number, -inner, 0).start())
+        pl.when(is_end)(lambda: dispatch(z, number, inner, 1).start())
         return carry
 
     lax.fori_loop(0, CHUNKS, send_own, 0)
+
+    def send_inner():
+        def step(number, carry):
+            dispatch(z, number, inner, 1).start()
+            return carry
+
+        pl.when(is_mid)(lambda: lax.fori_loop(0, CHUNKS, step, None))
 
     def place(flip):
         slots = (
@@ -348,13 +361,15 @@
 
     def near(number):
         arrive(1, 1, number)
-        pl.when(is_mid)(lambda: arrive(2, 3, number))
-
-    def next_near(number):
-        arrive(2 + mid, 2, number)
+
+    def mid_next(number):
+        pl.when(is_mid)(lambda: arrive(2, 2, number))
+
+    def across(number):
+        arrive(2 + mid, 3, number)
 
     def far(number):
-        pl.when(is_end)(lambda: arrive(3, 3, number))
+        pl.when(is_end)(lambda: arrive(3, 2, number))
 
     def gather(turn):
         def step(number, carry):
@@ -384,13 +399,14 @@
 
     def second(turn, begin, end):
         def step(number, carry):
-            part[turn, :, cols(number)] = jnp.dot(
-                hidden[...], down_w[:, cols(number)], preferred_element_type=jnp.float32
+            part[turn, :, pairs(number)] = jnp.dot(
+                hidden[...], down_w[:, pairs(number)], preferred_element_type=jnp.float32
             ).astype(jnp.bfloat16)
-            share_copy(turn, number).start()
+            share_copy(turn, 2 * number).start()
+            share_copy(turn, 2 * number + 1).start()
             return carry
 
-        lax.fori_loop(begin, end, step, 0)
+        lax.fori_loop(begin // 2, end // 2, step, 0)
 
     def third(turn, begin, end):
         def step(number, carry):
@@ -436,21 +452,23 @@
             step(*rest)
 
     G, F, U, T, C = gather, first, second, third, end_chain
-    A, B, E = near, next_near, far
+    A, M, B, E = near, mid_next, across, far
     for number in range(CHUNKS):
         select(0, 0, own, number)
     for flip in range(1, PLANES):
         routings[flip - 1].wait_recv()
         place(flip)
-    run((A, 0), (A, 1), (A, 2), (A, 3), (G, 0), (F, 0, 0, 8))
-    run((A, 4), (A, 5), (U, 0, 0, 4), (A, 6), (U, 0, 4, 8), (A, 7), (B, 0))
-    run((G, 1), (F, 1, 0, 4), (B, 1), (B, 2), (F, 1, 4, 8), (B, 3), (U, 1, 0, 4), (B, 4))
-    run((U, 1, 4, 8), (B, 5), (T, 1, 0, 4), (B, 6), (T, 1, 4, 6), (B, 7), (T, 1, 6, 8), (C, 1, 0))
-    run((E, 0), (C, 1, 1), (C, 1, 2), (E, 1), (C, 1, 3), (C, 1, 4), (G, 2), (F, 2, 0, 4), (E, 2))
-    run((E, 3), (C, 1, 5), (C, 1, 6), (C, 1, 7), (F, 2, 4, 8), (E, 4), (U, 2, 0, 4), (E, 5))
-    run((U, 2, 4, 8), (T, 2, 0, 2), (E, 6), (T, 2, 2, 4), (E, 7), (T, 2, 4, 8), (C, 2, 0), (C, 2, 1))
-    run((C, 2, 2), (C, 2, 3), (G, 3), (F, 3, 0, 4), (C, 2, 4), (C, 2, 5), (C, 2, 6), (C, 2, 7))
-    run((F, 3, 4, 8), (U, 3, 0, 4), (U, 3, 4, 8), (T, 3, 0, 8), (T, 0, 0, 8))
+    run((A, 0), (A, 1), (A, 2), (M, 0), (A, 3), (M, 1), (G, 0), (F, 0, 0, 8))
+    run((A, 4), (M, 2), (A, 5), (M, 3), (U, 0, 0, 4), (A, 6), (M, 4), (U, 0, 4, 8), (A, 7))
+    run((send_inner,), (M, 5), (B, 0), (M, 6), (M, 7))
+    run((G, 1), (F, 1, 0, 4), (B, 1), (B, 2), (F, 1, 4, 8), (B, 3), (U, 1, 0, 4), (U, 1, 4, 8))
+    run((B, 4), (T, 1, 0, 3), (B, 5), (T, 1, 3, 4), (B, 6), (T, 1, 4, 5), (C, 1, 0), (B, 7))
+    run((T, 1, 5, 6), (C, 1, 1), (C, 1, 2), (E, 0), (T, 1, 6, 8), (C, 1, 3), (E, 1), (G, 2))
+    run((F, 2, 0, 4), (C, 1, 4), (C, 1, 5), (E, 2), (E, 3), (F, 2, 4, 8), (U, 2, 0, 4), (C, 1, 6))
+    run((E, 4), (U, 2, 4, 8), (T, 2, 0, 2), (C, 1, 7), (E, 5), (E, 6), (T, 2, 2, 4), (E, 7))
+    run((T, 2, 4, 6), (C, 2, 0), (T, 2, 6, 8), (C, 2, 1), (C, 2, 2), (C, 2, 3), (G, 3), (F, 3, 0, 4))
+    run((C, 2, 4), (C, 2, 5), (F, 3, 4, 8), (U, 3, 0, 4), (C, 2, 6), (U, 3, 4, 8), (T, 3, 0, 4))
+    run((C, 2, 7), (T, 3, 4, 8), (T, 0, 0, 8))
     for number in range(CHUNKS):
         end_chain(3, number)
 
@@ -458,12 +476,12 @@
     def _():
         for number in range(CHUNKS):
             mid_link(2, number)
-        for number in range(CHUNKS):
-            mid_link(3, number)
             if number > 1:
                 mid_link(1, number - 2)
         mid_link(1, CHUNKS - 2)
         mid_link(1, CHUNKS - 1)
+        for number in range(CHUNKS):
+            mid_link(3, number)
 
     def finish(number, carry):
         total = after[:, cols(number)].astype(jnp.float32) + combined(0, number)
@@ -493,8 +511,8 @@
     exchange.wait_send()
     for copy in routings:
         copy.wait_send()
-    pl.when(has_left)(lambda: sent(own, disp_sent).wait_send())
-    pl.when(has_right)(lambda: sent(own, disp_sent.at[pl.ds(1, 1)]).wait_send())
+    pl.when(is_mid)(lambda: sent(own, disp_sent).wait_send())
+    sent(own, disp_sent.at[pl.ds(1, 1)]).wait_send()
     pl.when(is_mid)(
         lambda: sent(dense.at[pl.ds(0, PLANES - 1)], disp_sent.at[pl.ds(2, 1)]).wait_send()
     )

time: 128 us -> 120 us (0.938)
  the two profiles are of different devices: /device:TPU:0 before, /device:TPU:12 now
where the time goes in v5:
time: 120 us
  Pallas kernels  118 us (98%)
  local copies, waits for them, and re-layouts  2.09 us (2%)
    pallas_call x1, Pallas kernels, run_layer(): pl.pallas_call(functools.partial(layer_kernel, count, cap), out_shape=jax...  118 us

profile of v5, /device:TPU:12, one launch (start us, length us, event | category | flops | bytes accessed | tf_op | source)
XLA Modules:
  0.0 119.7 jit_solution(10693631968876369318)
XLA Ops:
  0.0 117.6 %shard_map.136 = bf16[192,2048]{1,0:T(8,128)(2,1)} custom-call(bf16[384,512]{1,0:T(8,128)(2,1)} %values.1, bf16[384,512]{1,0:T(8,128)(2,1)} %gates.1, f32[31,512]{1,0:T(8,128)} %taps.1, f32[1,512]{1,0:T(1,128)} %bitcast.7, f32[1,512]{1,0:T(1,128)} %bitcast.8, f32[1,512]{1,0:T(1,128)} %bitcast.9, f32[1,2048]{1,0:T(1,128)} %bitcast.6, s32[2,192]{1,0:T(2,128)} %bitcast.10, ...), custom_call_target="tpu_custom_call" | custom-call | tf_op jit(solution)/shard_map/pallas_call | solution.py:542
  117.6 2.1 %copy.16 = bf16[192,2048]{1,0:T(8,128)(2,1)} copy(bf16[192,2048]{1,0:T(8,128)(2,1)} %shard_map.136) | data formatting | bytes 1572864

commit v6 on v5

--- a/solution.py
+++ b/solution.py
@@ -25,7 +25,7 @@
     count, cap, values, gates, taps, bias, gain, shift, norm_gain, ids, scales,
     residual_in, mix_in, gate_in, up_in, down_in, out,
     dense, pick, rows, part, given, hidden, ret, zout, zin, gate_w, up_w, down_w,
-    extended, mixed, tail, stats, swapped, acted, route, picks, weights,
+    extended, mixed, tail, stats, swapped, acted, route, picks, weights, projected,
     disp_sent, disp_came, plane_sent, plane_came, pair_sent, pair_came, part_sent, part_came,
     back_sent, back_came, chain_sent, chain_came, loaded, mix_sent, mix_came,
 ):
@@ -296,12 +296,24 @@
     activate(core, store_mine)
     for load in early:
         load.wait()
+    ours = pl.ds(pl.multiple_of(core * chan, chan), chan)
+    theirs = pl.ds(pl.multiple_of(other * chan, chan), chan)
+
+    def half_project(number, carry):
+        projected[:, pairs(number)] = after[:, pairs(number)].astype(jnp.float32) + jnp.dot(
+            acted[:, ours], down_w[ours, pairs(number)], preferred_element_type=jnp.float32
+        )
+        return carry
+
+    lax.fori_loop(0, CHUNKS // 2, half_project, 0)
     exchange.wait_recv()
 
     def project(number, carry):
         block = (
-            after[:, pairs(number)].astype(jnp.float32)
-            + jnp.dot(acted[...], down_w[:, pairs(number)], preferred_element_type=jnp.float32)
+            projected[:, pairs(number)]
+            + jnp.dot(
+                acted[:, theirs], down_w[theirs, pairs(number)], preferred_element_type=jnp.float32
+            )
         ).astype(jnp.bfloat16)
         after[:, pairs(number)] = block
         wider = block.astype(jnp.float32)
@@ -453,6 +465,10 @@
 
     G, F, U, T, C = gather, first, second, third, end_chain
     A, M, B, E = near, mid_next, across, far
+
+    def R(turn, number):
+        pl.when(is_mid)(lambda: mid_link(turn, number))
+
     for number in range(CHUNKS):
         select(0, 0, own, number)
     for flip in range(1, PLANES):
@@ -460,28 +476,29 @@
         place(flip)
     run((A, 0), (A, 1), (A, 2), (M, 0), (A, 3), (M, 1), (G, 0), (F, 0, 0, 8))
     run((A, 4), (M, 2), (A, 5), (M, 3), (U, 0, 0, 4), (A, 6), (M, 4), (U, 0, 4, 8), (A, 7))
-    run((send_inner,), (M, 5), (B, 0), (M, 6), (M, 7))
-    run((G, 1), (F, 1, 0, 4), (B, 1), (B, 2), (F, 1, 4, 8), (B, 3), (U, 1, 0, 4), (U, 1, 4, 8))
-    run((B, 4), (T, 1, 0, 3), (B, 5), (T, 1, 3, 4), (B, 6), (T, 1, 4, 5), (C, 1, 0), (B, 7))
+    run((send_inner,), (M, 5), (M, 6), (M, 7), (G, 1), (F, 1, 0, 4), (B, 0), (B, 1), (B, 2))
+    run((F, 1, 4, 8), (B, 3), (U, 1, 0, 4), (B, 4), (T, 1, 0, 2), (U, 1, 4, 8), (T, 1, 2, 3), (B, 5))
+    run((T, 1, 3, 4), (B, 6), (T, 1, 4, 5), (C, 1, 0), (B, 7))
     run((T, 1, 5, 6), (C, 1, 1), (C, 1, 2), (E, 0), (T, 1, 6, 8), (C, 1, 3), (E, 1), (G, 2))
     run((F, 2, 0, 4), (C, 1, 4), (C, 1, 5), (E, 2), (E, 3), (F, 2, 4, 8), (U, 2, 0, 4), (C, 1, 6))
-    run((E, 4), (U, 2, 4, 8), (T, 2, 0, 2), (C, 1, 7), (E, 5), (E, 6), (T, 2, 2, 4), (E, 7))
+    run((E, 4), (T, 2, 0, 2), (U, 2, 4, 8), (T, 2, 2, 4), (C, 1, 7), (E, 5), (E, 6), (E, 7))
     run((T, 2, 4, 6), (C, 2, 0), (T, 2, 6, 8), (C, 2, 1), (C, 2, 2), (C, 2, 3), (G, 3), (F, 3, 0, 4))
-    run((C, 2, 4), (C, 2, 5), (F, 3, 4, 8), (U, 3, 0, 4), (C, 2, 6), (U, 3, 4, 8), (T, 3, 0, 4))
-    run((C, 2, 7), (T, 3, 4, 8), (T, 0, 0, 8))
+    run((C, 2, 4), (C, 2, 5), (F, 3, 4, 8), (R, 2, 0), (U, 3, 0, 4))
+    run((C, 2, 6), (T, 3, 0, 2), (R, 2, 1), (U, 3, 4, 8), (T, 3, 2, 4), (C, 2, 7), (T, 3, 4, 8))
+    run((R, 2, 2), (T, 0, 0, 8))
     for number in range(CHUNKS):
         end_chain(3, number)
 
     @pl.when(is_mid)
     def _():
         for number in range(CHUNKS):
-            mid_link(2, number)
-            if number > 1:
-                mid_link(1, number - 2)
-        mid_link(1, CHUNKS - 2)
-        mid_link(1, CHUNKS - 1)
+            if number > 2:
+                mid_link(2, number)
+                mid_link(1, number - 3)
         for number in range(CHUNKS):
             mid_link(3, number)
+            if number < 3:
+                mid_link(1, CHUNKS - 3 + number)
 
     def finish(number, carry):
         total = after[:, cols(number)].astype(jnp.float32) + combined(0, number)
@@ -566,6 +583,7 @@
             pltpu.VMEM((PLANES, 2 * choose_count, row_count), jnp.float32),
             pltpu.VMEM((PLANES, half, row_count), held),
             pltpu.VMEM((PLANES, 2, half, row_count), held),
+            pltpu.VMEM((row_count, width), jnp.float32),
             dma(3), dma(PLANES, CHUNKS),
             dma(1), dma(PLANES, CHUNKS),
             dma(1), dma(PLANES),

time: 120 us -> 115 us (0.958)
  the two profiles are of different devices: /device:TPU:12 before, /device:TPU:13 now
where the time goes in v6:
time: 115 us
  Pallas kernels  113 us (98%)
  local copies, waits for them, and re-layouts  2.09 us (2%)
    pallas_call x1, Pallas kernels, run_layer(): pl.pallas_call(functools.partial(layer_kernel, count, cap), out_shape=jax...  113 us

profile of v6, /device:TPU:13, one launch (start us, length us, event | category | flops | bytes accessed | tf_op | source)
XLA Modules:
  0.0 114.9 jit_solution(18178613358423058129)
XLA Ops:
  0.0 112.8 %shard_map.136 = bf16[192,2048]{1,0:T(8,128)(2,1)} custom-call(bf16[384,512]{1,0:T(8,128)(2,1)} %values.1, bf16[384,512]{1,0:T(8,128)(2,1)} %gates.1, f32[31,512]{1,0:T(8,128)} %taps.1, f32[1,512]{1,0:T(1,128)} %bitcast.7, f32[1,512]{1,0:T(1,128)} %bitcast.8, f32[1,512]{1,0:T(1,128)} %bitcast.9, f32[1,2048]{1,0:T(1,128)} %bitcast.6, s32[2,192]{1,0:T(2,128)} %bitcast.10, ...), custom_call_target="tpu_custom_call" | custom-call | tf_op jit(solution)/shard_map/pallas_call | solution.py:559
  112.8 2.1 %copy.16 = bf16[192,2048]{1,0:T(8,128)(2,1)} copy(bf16[192,2048]{1,0:T(8,128)(2,1)} %shard_map.136) | data formatting | bytes 1572864

commit v7 on v6

--- a/solution.py
+++ b/solution.py
@@ -481,8 +481,8 @@
     run((T, 1, 3, 4), (B, 6), (T, 1, 4, 5), (C, 1, 0), (B, 7))
     run((T, 1, 5, 6), (C, 1, 1), (C, 1, 2), (E, 0), (T, 1, 6, 8), (C, 1, 3), (E, 1), (G, 2))
     run((F, 2, 0, 4), (C, 1, 4), (C, 1, 5), (E, 2), (E, 3), (F, 2, 4, 8), (U, 2, 0, 4), (C, 1, 6))
-    run((E, 4), (T, 2, 0, 2), (U, 2, 4, 8), (T, 2, 2, 4), (C, 1, 7), (E, 5), (E, 6), (E, 7))
-    run((T, 2, 4, 6), (C, 2, 0), (T, 2, 6, 8), (C, 2, 1), (C, 2, 2), (C, 2, 3), (G, 3), (F, 3, 0, 4))
+    run((E, 4), (T, 2, 0, 2), (U, 2, 4, 8), (C, 1, 7), (E, 5), (E, 6), (E, 7))
+    run((T, 2, 2, 6), (C, 2, 0), (T, 2, 6, 8), (C, 2, 1), (C, 2, 2), (C, 2, 3), (G, 3), (F, 3, 0, 4))
     run((C, 2, 4), (C, 2, 5), (F, 3, 4, 8), (R, 2, 0), (U, 3, 0, 4))
     run((C, 2, 6), (T, 3, 0, 2), (R, 2, 1), (U, 3, 4, 8), (T, 3, 2, 4), (C, 2, 7), (T, 3, 4, 8))
     run((R, 2, 2), (T, 0, 0, 8))

time: 115 us -> 115 us (level)
  the two profiles are of different devices: /device:TPU:13 before, /device:TPU:12 now
where the time goes in v7:
time: 115 us
  Pallas kernels  113 us (98%)
  local copies, waits for them, and re-layouts  2.09 us (2%)
    pallas_call x1, Pallas kernels, run_layer(): pl.pallas_call(functools.partial(layer_kernel, count, cap), out_shape=jax...  113 us

profile of v7, /device:TPU:12, one launch (start us, length us, event | category | flops | bytes accessed | tf_op | source)
XLA Modules:
  0.0 115.0 jit_solution(10489313659482331244)
XLA Ops:
  0.0 112.9 %shard_map.136 = bf16[192,2048]{1,0:T(8,128)(2,1)} custom-call(bf16[384,512]{1,0:T(8,128)(2,1)} %values.1, bf16[384,512]{1,0:T(8,128)(2,1)} %gates.1, f32[31,512]{1,0:T(8,128)} %taps.1, f32[1,512]{1,0:T(1,128)} %bitcast.7, f32[1,512]{1,0:T(1,128)} %bitcast.8, f32[1,512]{1,0:T(1,128)} %bitcast.9, f32[1,2048]{1,0:T(1,128)} %bitcast.6, s32[2,192]{1,0:T(2,128)} %bitcast.10, ...), custom_call_target="tpu_custom_call" | custom-call | tf_op jit(solution)/shard_map/pallas_call | solution.py:559
  112.9 2.1 %copy.16 = bf16[192,2048]{1,0:T(8,128)(2,1)} copy(bf16[192,2048]{1,0:T(8,128)(2,1)} %shard_map.136) | data formatting | bytes 1572864
